TPU v7x, 32 devices: a whole 2x2x4 slice. The times are simulated.
32 devices in a mesh: grp: 2 (over x), ep: 8 (over z, y), tp: 2 (over core).
Axes of the slice: x: 2, y: 2, z: 4, core: 2. Of those that a mesh axis runs over, the one named last changes fastest.
Arguments:
- tokens: bfloat16 [8192, 2048], P(('grp', 'ep', 'tp')), parts along dimension 0, may hold values from -6 to 6
- norm_gain: float32 [2048], replicated, may hold values from 0.1 to 1.9
- expert_ids: int32 [8192, 2], P(('grp', 'ep', 'tp')), parts along dimension 0, may hold values from 0 to 15, all different within a row; in each aligned block of 256 rows (0 to 255, 256 to 511, ...) at most 64 rows name the same one
- gate_values: float32 [8192, 2], P(('grp', 'ep', 'tp')), parts along dimension 0, may hold values from 0.2 to 2
- w_gate: bfloat16 [16, 2048, 512], P('ep', None, 'tp'), may hold values from -0.125 to 0.125
- w_up: bfloat16 [16, 2048, 512], P('ep', None, 'tp'), may hold values from -0.125 to 0.125
- w_down: bfloat16 [16, 512, 2048], P('ep', 'tp'), may hold values from -0.25 to 0.25
- s_gate: bfloat16 [2048, 512], P(None, 'tp'), may hold values from -0.125 to 0.125
- s_up: bfloat16 [2048, 512], P(None, 'tp'), may hold values from -0.125 to 0.125
- s_down: bfloat16 [512, 2048], P('tp'), may hold values from -0.25 to 0.25
Outputs:
- mixed: bfloat16 [8192, 2048], P(('grp', 'ep', 'tp')), parts along dimension 0
There are 2 independent parts, one for each index of `grp`. A program takes and returns all parts, laid end to end along the dimension named above; an argument that names none is the same for every part. Nothing has to cross between parts.
Inputs may be any that keep to these rules, and one draw needn't show every extreme that they name: `expert_ids`: each row names 2 different experts. Within the rows of one device no expert is named by more than 64 rows, a bound that some block reaches.
All inputs are finite; a program needn't handle non-finite values.
Results may differ from a plain program's by a relative error of at most 0.0068.
Values may be sent and summed in bfloat16 or wider, within the bound.
No kernel may reach another device: no remote copies, remote signals or barrier semaphores. Data moves between devices by JAX's collectives and lax.ppermute only.
A program may use at most 128 MiB of HBM per device.

v0:
```python
import jax
import jax.numpy as jnp
from jax import lax
from jax.sharding import PartitionSpec as P


def swiglu_rows(rows, first_w, second_w):
    first = jnp.einsum("xecd,edf->xecf", rows, first_w, preferred_element_type=jnp.float32)
    second = jnp.einsum("xecd,edf->xecf", rows, second_w, preferred_element_type=jnp.float32)
    return (jax.nn.silu(first) * second).astype(jnp.bfloat16)


def shared_swiglu(rows, first_w, second_w):
    first = jnp.dot(rows, first_w, preferred_element_type=jnp.float32)
    second = jnp.dot(rows, second_w, preferred_element_type=jnp.float32)
    return (jax.nn.silu(first) * second).astype(jnp.bfloat16)


def body(tokens, norm_gain, expert_ids, gate_values, w_gate, w_up, w_down, s_gate, s_up, s_down):
    n_rows, width = tokens.shape
    topk = expert_ids.shape[1]
    ep_size = lax.axis_size("ep")
    local_exp = w_gate.shape[0]
    experts_n = local_exp * ep_size
    capacity = 2 * n_rows * topk // experts_n
    xf = tokens.astype(jnp.float32)
    scale = lax.rsqrt(jnp.mean(xf * xf, axis=-1, keepdims=True) + 1e-06)
    normed = (xf * scale * norm_gain).astype(jnp.bfloat16)
    s_hidden = shared_swiglu(lax.all_gather(normed, "tp", axis=0, tiled=True), s_gate, s_up)
    shared = lax.psum_scatter(
        jnp.dot(s_hidden, s_down, preferred_element_type=jnp.float32),
        "tp",
        scatter_dimension=0,
        tiled=True,
    )
    flat_e = expert_ids.reshape(-1)
    onehot = (flat_e[:, None] == jnp.arange(experts_n, dtype=jnp.int32)[None, :]).astype(jnp.int32)
    before = jnp.cumsum(onehot, axis=0) - onehot
    slot = jnp.sum(before * onehot, axis=1)
    position = flat_e * capacity + slot
    flat_tok = jnp.arange(flat_e.shape[0], dtype=jnp.int32) // topk
    slot_tok = jnp.full((experts_n * capacity,), n_rows, jnp.int32).at[position].set(flat_tok)
    padded = jnp.concatenate([normed, jnp.zeros((1, width), jnp.bfloat16)], axis=0)
    outgoing = padded[slot_tok].reshape(ep_size, local_exp, capacity, width)
    arrived = lax.all_to_all(outgoing, "ep", split_axis=0, concat_axis=0, tiled=True)
    full_gate, full_up = (
        lax.all_gather(w_gate, "tp", axis=2, tiled=True),
        lax.all_gather(w_up, "tp", axis=2, tiled=True),
    )
    full_down = lax.all_gather(w_down, "tp", axis=1, tiled=True)
    hidden = swiglu_rows(arrived, full_gate, full_up)
    results = jnp.einsum("xecf,efd->xecd", hidden, full_down, preferred_element_type=jnp.float32)
    returned = lax.all_to_all(
        results.astype(jnp.bfloat16), "ep", split_axis=0, concat_axis=0, tiled=True
    )
    picked = returned.reshape(experts_n * capacity, width)[position].reshape(n_rows, topk, width)
    routed = jnp.sum(gate_values[:, :, None] * picked.astype(jnp.float32), axis=1)
    return (shared + routed).astype(jnp.bfloat16)


def solution(mesh):
    return jax.shard_map(
        body,
        mesh=mesh,
        in_specs=(
            P(("grp", "ep", "tp"), None),
            P(),
            P(("grp", "ep", "tp"), None),
            P(("grp", "ep", "tp"), None),
            P("ep", None, "tp"),
            P("ep", None, "tp"),
            P("ep", "tp", None),
            P(None, "tp"),
            P(None, "tp"),
            P("tp", None),
        ),
        out_specs=P(("grp", "ep", "tp"), None),
        check_vma=False,
    )
```

profile of v0, /device:TPU:0, one launch (start us, length us, event | category | flops | bytes accessed | tf_op | source)
XLA Modules:
  0.0 272.1 jit_solution(9954740168588440158)
XLA Ops:
  6.5 1.6 fusion.10
  8.1 2.5 fusion.12
  10.8 0.7 all-gather.7.cloned.1.call-update
  11.5 0.7 all-gather.11.cloned.1.call-update
  12.3 0.1 eq.29
  12.6 1.2 reduce-window.6
  13.8 0.2 slice_reduce_fusion
  14.2 0.2 mul.70
  14.6 2.4 scatter_custom_fusion
  17.1 6.0 %gather_fusion = bf16[1024,2048]{1,0:T(8,128)(2,1)} fusion(bf16[257,2048]{1,0:T(8,128)(2,1)S(1)} %concatenate.3, s32[1024]{0:T(1024)S(1)} %fusion.38), kind=kCustom, calls=%fused_computation | custom fusion | bytes 8392704 | tf_op jit(solution)/shard_map/gather | solution.py:44
  23.1 7.3 %all-to-all-start = ((bf16[8,2,64,2048]{3,2,1,0:T(8,128)(2,1)}), bf16[8,2,64,2048]{3,2,1,0:T(8,128)(2,1)}, u32[]{:S(2)}, u32[]{:S(2)}) async-start(bf16[8,2,64,2048]{3,2,1,0:T(8,128)(2,1)} %bitcast.72), calls=%async_computation.1 | async-start | bytes 8388608 | tf_op jit(solution)/shard_map/all_to_all | solution.py:45
  30.5 0.5 all-gather.9.cloned.1.call-update
  31.1 3.7 %fusion.46 = f32[512,256]{1,0:T(8,128)} fusion(bf16[512,2048]{1,0:T(8,128)(2,1)} %all-gather.5.cloned.1.call-done, bf16[2048,256]{1,0:T(8,128)(2,1)} %param.17), kind=kOutput, calls=%fused_computation.62 | convolution fusion | flops 536870912 | bytes 3670016 | tf_op jit(solution)/shard_map/dot_general | solution.py:14
  34.8 5.8 %fusion.26 = f32[512,2048]{1,0:T(8,128)} fusion(bf16[256,2048]{1,0:T(8,128)(2,1)S(1)} %copy-done, bf16[512,2048]{1,0:T(8,128)(2,1)S(1)} %copy-done.3, bf16[2048,256]{1,0:T(8,128)(2,1)} %param.18, f32[512,256]{1,0:T(8,128)} %fusion.46), kind=kOutput, calls=%fused_computation.28 | convolution fusion | flops 1074528256 | bytes 8912896 | tf_op jit(solution)/shard_map/dot_general | solution.py:31
  40.7 83.0 %all-to-all-done = bf16[8,2,64,2048]{3,2,1,0:T(8,128)(2,1)} async-done(((bf16[8,2,64,2048]{3,2,1,0:T(8,128)(2,1)}), bf16[8,2,64,2048]{3,2,1,0:T(8,128)(2,1)}, u32[]{:S(2)}, u32[]{:S(2)}) %all-to-all-start) | async-done | bytes 4194336 | tf_op jit(solution)/shard_map/all_to_all | solution.py:45
  123.7 5.8 %fusion.4 = f32[2,8,64,512]{3,2,1,0:T(8,128)S(1)} fusion(bf16[2,2048,512]{2,1,0:T(8,128)(2,1)} %all-gather.7.cloned.1.call-done, bf16[8,2,64,2048]{3,2,1,0:T(8,128)(2,1)} %all-to-all-done), kind=kOutput, calls=%fused_computation.7 | convolution fusion | flops 2147483648 | bytes 10485760 | tf_op jit(solution)/shard_map/xecd,edf->xecf/dot_general | solution.py:8
  129.5 11.2 %convert_bitcast_fusion = bf16[8,2,64,2048]{3,2,0,1:T(8,128)(2,1)} fusion(bf16[2,512,2048]{2,1,0:T(8,128)(2,1)} %all-gather.11.cloned.1.call-done, f32[2,8,64,512]{3,2,1,0:T(8,128)S(1)} %fusion.4, bf16[2,2048,512]{2,1,0:T(8,128)(2,1)} %all-gather.9.cloned.1.call-done, bf16[8,2,64,2048]{3,2,1,0:T(8,128)(2,1)} %all-to-all-done), kind=kOutput, calls=%fused_computation.10 | convolution fusion | flops 4300210176 | bytes 18874368 | tf_op jit(solution)/shard_map/xecf,efd->xecd/dot_general | solution.py:52
  140.7 4.7 %copy.26 = bf16[8,2,64,2048]{3,2,1,0:T(8,128)(2,1)} copy(bf16[8,2,64,2048]{3,2,0,1:T(8,128)(2,1)} %convert_bitcast_fusion) | data formatting | bytes 8388608 | tf_op jit(solution)/shard_map/convert_element_type | solution.py:54
  145.5 4.9 %all-to-all-start.1 = ((bf16[8,2,64,2048]{3,2,1,0:T(8,128)(2,1)}), bf16[8,2,64,2048]{3,2,1,0:T(8,128)(2,1)}, u32[]{:S(2)}, u32[]{:S(2)}) async-start(bf16[8,2,64,2048]{3,2,1,0:T(8,128)(2,1)} %copy.26), calls=%async_computation.2 | async-start | bytes 8388608 | tf_op jit(solution)/shard_map/all_to_all | solution.py:53
  150.6 92.2 %all-to-all-done.1 = bf16[8,2,64,2048]{3,2,1,0:T(8,128)(2,1)} async-done(((bf16[8,2,64,2048]{3,2,1,0:T(8,128)(2,1)}), bf16[8,2,64,2048]{3,2,1,0:T(8,128)(2,1)}, u32[]{:S(2)}, u32[]{:S(2)}) %all-to-all-start.1) | async-done | bytes 4194336 | tf_op jit(solution)/shard_map/all_to_all | solution.py:53
  242.7 7.1 %gather_fusion.1 = bf16[512,2048]{1,0:T(8,128)(2,1)S(1)} fusion(bf16[1024,2048]{1,0:T(8,128)(2,1)} %bitcast.13, s32[1024]{0:T(1024)S(1)} %pad_clamp_fusion), kind=kCustom, calls=%fused_computation.1 | custom fusion | bytes 4196352 | tf_op jit(solution)/shard_map/gather | solution.py:56
  249.9 4.0 %reshape.68 = f32[256,2,2048]{2,1,0:T(2,128)} reshape(bf16[512,2048]{1,0:T(8,128)(2,1)S(1)} %gather_fusion.1) | data formatting | bytes 6291456 | tf_op jit(solution)/shard_map/convert_element_type | solution.py:57
  253.9 8.9 %multiply_reduce_fusion = f32[256,2048]{1,0:T(8,128)S(1)} fusion(f32[256,2,2048]{2,1,0:T(2,128)} %reshape.68, f32[256,2]{1,0:T(8,128)S(1)} %copy.19), kind=kLoop, calls=%fused_computation.9 | loop fusion | flops 1572864 | bytes 6293504 | tf_op jit(solution)/shard_map/reduce_sum | solution.py:57
  262.8 2.8 %add_convert_fusion = bf16[256,2048]{1,0:T(8,128)(2,1)} fusion(f32[256,2048]{1,0:T(8,128)} %reduce-scatter.2.cloned.1.call-done, f32[256,2048]{1,0:T(8,128)S(1)} %multiply_reduce_fusion), kind=kLoop, calls=%fused_computation.25 | loop fusion | flops 1048576 | bytes 5242880 | tf_op jit(solution)/shard_map/convert_element_type | solution.py:58
  (39 shorter events, 1.1 us)
Async XLA Ops:
  6.5 28.3 %copy-start = (bf16[256,2048]{1,0:T(8,128)(2,1)S(1)}, bf16[256,2048]{1,0:T(8,128)(2,1)}, u32[]{:S(2)}) copy-start(bf16[256,2048]{1,0:T(8,128)(2,1)} %param.19) | copy-start | bytes 3145732
  6.5 24.5 %all-gather.5.cloned.1.call-start = ((), (), s32[]{:S(2)}) async-start(), calls=%async_computation.3 | async-start | bytes 3145728 | tf_op jit(solution)/shard_map/all_gather | solution.py:29
  10.7 1.5 copy-start.4
  10.7 3.7 %copy-start.2 = (bf16[256,2048]{1,0:T(8,128)(2,1)S(1)}, bf16[256,2048]{1,0:T(8,128)(2,1)}, u32[]{:S(2)}) copy-start(bf16[256,2048]{1,0:T(8,128)(2,1)} %fusion.12) | copy-start | bytes 3145732
  10.7 30.0 %all-gather.7.cloned.1.call-start = ((), (), s32[]{:S(2)}) async-start(), calls=%async_computation.5 | async-start | bytes 6291456 | tf_op jit(solution)/shard_map/all_gather | solution.py:47
  11.5 118.1 %all-gather.11.cloned.1.call-start = ((), (), s32[]{:S(2)}) async-start(), calls=%async_computation.7 | async-start | bytes 6291456 | tf_op jit(solution)/shard_map/all_gather | solution.py:50
  23.1 100.6 %all-to-all-start = ((bf16[8,2,64,2048]{3,2,1,0:T(8,128)(2,1)}), bf16[8,2,64,2048]{3,2,1,0:T(8,128)(2,1)}, u32[]{:S(2)}, u32[]{:S(2)}) async-start(bf16[8,2,64,2048]{3,2,1,0:T(8,128)(2,1)} %bitcast.72), calls=%async_computation.1 | async-start | bytes 8388608 | tf_op jit(solution)/shard_map/all_to_all | solution.py:45
  30.4 99.1 %all-gather.9.cloned.1.call-start = ((), (), s32[]{:S(2)}) async-start(), calls=%async_computation.6 | async-start | bytes 6291456 | tf_op jit(solution)/shard_map/all_gather | solution.py:48
  31.0 231.8 %reduce-scatter.2.cloned.1.call-start = ((), (), s32[]{:S(2)}) async-start(), calls=%async_computation.4 | async-start | bytes 6291456 | tf_op jit(solution)/shard_map/reduce_scatter | solution.py:30
  31.1 3.7 %copy-start.3 = (bf16[512,2048]{1,0:T(8,128)(2,1)S(1)}, bf16[512,2048]{1,0:T(8,128)(2,1)}, u32[]{:S(2)}) copy-start(bf16[512,2048]{1,0:T(8,128)(2,1)} %all-gather.5.cloned.1.call-done) | copy-start | bytes 6291460
  145.5 4.9 %copy-start.5 = (f32[256,2]{0,1:T(2,128)S(1)}, f32[256,2]{0,1:T(2,128)}, u32[]{:S(2)}) copy-start(f32[256,2]{0,1:T(2,128)} %param.13) | copy-start | bytes 6148
  145.5 97.3 %all-to-all-start.1 = ((bf16[8,2,64,2048]{3,2,1,0:T(8,128)(2,1)}), bf16[8,2,64,2048]{3,2,1,0:T(8,128)(2,1)}, u32[]{:S(2)}, u32[]{:S(2)}) async-start(bf16[8,2,64,2048]{3,2,1,0:T(8,128)(2,1)} %copy.26), calls=%async_computation.2 | async-start | bytes 8388608 | tf_op jit(solution)/shard_map/all_to_all | solution.py:53
  253.9 11.7 %copy-start.1 = (bf16[256,2048]{1,0:T(8,128)(2,1)S(1)}, bf16[256,2048]{1,0:T(8,128)(2,1)}, u32[]{:S(2)}) copy-start(bf16[256,2048]{1,0:T(8,128)(2,1)} %param.19) | copy-start | bytes 3145732
Sparse Core Ops, SparseCore 0:
  10.8 13.2 all-gather.4
  25.7 13.9 all-gather.6
  41.2 14.8 all-gather.10
  57.5 13.9 all-gather.8
  73.6 13.2 reduce-scatter.1
where the time goes:
time: 273 us; the launch traced here: 272 us
  waiting for transfers between devices  177 us (65%)
  matrix products  26.6 us (10%)
  local copies, waits for them, and re-layouts  25.5 us (9%)
  other arithmetic  17.1 us (6%)
  between operations  13.3 us (5%)
  starting transfers between devices  12.4 us (5%)
    all_to_all x1, waiting for transfers between devices, body(): lax.all_to_all(results.astype(jnp.bfloat16), 'ep', split_axis=0, concat_a...  92.2 us
    all_to_all x1, waiting for transfers between devices, body(): lax.all_to_all(outgoing, 'ep', split_axis=0, concat_axis=0, tiled=True)  83 us
    dot_general x1, matrix products, body(): jnp.einsum('xecf,efd->xecd', hidden, full_down, preferred_element_type=jn...  11.2 us
    reduce_sum x1, other arithmetic, body(): jnp.sum(gate_values[:, :, None] * picked.astype(jnp.float32), axis=1)  8.86 us
    all_to_all x1, starting transfers between devices, body(): lax.all_to_all(outgoing, 'ep', split_axis=0, concat_axis=0, tiled=True)  7.31 us
    gather x1, local copies, waits for them, and re-layouts, body(): returned.reshape(experts_n * capacity, width)[position]  7.13 us
    gather x1, local copies, waits for them, and re-layouts, body(): outgoing = padded[slot_tok].reshape(ep_size, local_exp, capacity, width)  6.04 us
    dot_general x1, matrix products, body(): jnp.dot(s_hidden, s_down, preferred_element_type=jnp.float32)  5.85 us
  transfers between devices with their start and end apart: 7, of which 2 were waited for; matrix products, arithmetic and copies ran while one was open for 23% of the time, Pallas kernels for 0%

commit v1 on v0

v1 whole, which is shorter than its diff:
```python
import functools

import jax
import jax.numpy as jnp
from jax import lax
from jax.experimental import pallas as pl
from jax.experimental.pallas import tpu as pltpu
from jax.sharding import PartitionSpec as P


CHUNKS = 4
SMALL = pltpu.CompilerParams(vmem_limit_bytes=8 * 1024 * 1024)
LARGE = pltpu.CompilerParams(vmem_limit_bytes=16 * 1024 * 1024)
BF, F32 = jnp.bfloat16, jnp.float32


def cost(flops, nbytes):
    return pl.CostEstimate(flops=int(flops), bytes_accessed=int(nbytes), transcendentals=0)


def route(meta, experts, topk, cap, weighted):
    n = meta.shape[1]
    count = experts.shape[0]
    same = [jnp.broadcast_to(meta[k : k + 1, :], (count, n)) == experts for k in range(topk)]
    marks = functools.reduce(jnp.logical_or, same)
    before = lax.broadcasted_iota(jnp.int32, (n, n), 0) < lax.broadcasted_iota(jnp.int32, (n, n), 1)
    rank = jnp.dot(marks.astype(F32).astype(BF), before.astype(F32).astype(BF), preferred_element_type=F32)
    keys = jnp.where(marks, rank, -1.0)
    slot = lax.broadcasted_iota(jnp.int32, (cap, n), 0).astype(F32)
    hits = [jnp.broadcast_to(keys[r : r + 1, :], (cap, n)) == slot for r in range(count)]
    if not weighted:
        return jnp.concatenate([h.astype(F32) for h in hits], axis=0).astype(BF)
    gates = sum(jnp.where(same[k], jnp.broadcast_to(meta[topk + k : topk + k + 1, :], (count, n)), 0.0) for k in range(topk))
    high, low = [], []
    for r, hit in enumerate(hits):
        w = jnp.where(hit, jnp.broadcast_to(gates[r : r + 1, :], (cap, n)), 0.0)
        top = w.astype(BF)
        high.append(top)
        low.append((w - top.astype(F32)).astype(BF))
    return jnp.concatenate(high, axis=0), jnp.concatenate(low, axis=0)


def compact(block, meta, experts, topk, local_exp, cap):
    n, d = block.shape
    groups = experts.shape[0] // local_exp
    rows = local_exp * cap
    steps = 2
    wide = d // steps

    def kernel(x_ref, m_ref, e_ref, *refs):
        outs, onehot = refs[:-1], refs[-1]

        @pl.when(pl.program_id(0) == 0)
        def _():
            onehot[...] = route(m_ref[...], e_ref[...], topk, cap, False)

        picked = jnp.dot(onehot[...], x_ref[...], preferred_element_type=F32).astype(BF)
        for g in range(groups):
            outs[g][...] = picked[g * rows : (g + 1) * rows]

    return pl.pallas_call(
        kernel,
        grid=(steps,),
        in_specs=[
            pl.BlockSpec((n, wide), lambda i: (0, i)),
            pl.BlockSpec(meta.shape, lambda i: (0, 0)),
            pl.BlockSpec(experts.shape, lambda i: (0, 0)),
        ],
        out_specs=[pl.BlockSpec((rows, wide), lambda i: (0, i))] * groups,
        out_shape=[jax.ShapeDtypeStruct((rows, d), BF)] * groups,
        scratch_shapes=[pltpu.VMEM((groups * rows, n), BF)],
        cost_estimate=cost(2e9, 2 * n * d * 2),
        compiler_params=SMALL,
        name="compact_rows",
    )(block, meta, experts)


def combine(meta, experts, topk, parts, cap, extra, dtype, pieces):
    groups = len(parts)
    n = meta.shape[1]
    d = parts[0].shape[1]
    wide = d // pieces

    def kernel(m_ref, e_ref, *refs):
        ins, outs = refs[:-pieces], refs[-pieces:]
        mats = route(m_ref[...], e_ref[...], topk, cap, True)
        for p in range(pieces):
            low = p * wide
            stacked = jnp.concatenate([r[:, low : low + wide] for r in ins[:groups]], axis=0)
            total = None
            for mat in mats:
                piece = lax.dot_general(mat, stacked, (((0,), (0,)), ((), ())), preferred_element_type=F32)
                total = piece if total is None else total + piece
            for more in ins[groups:]:
                total = total + more[:, low : low + wide].astype(F32)
            outs[p][...] = total.astype(dtype)

    return pl.pallas_call(
        kernel,
        out_shape=[jax.ShapeDtypeStruct((n, wide), dtype)] * pieces,
        cost_estimate=cost(1.5e9, 2 * n * d * 2),
        compiler_params=SMALL,
        name="combine_rows",
    )(meta, experts, *parts, *extra)


def combine_matrix(meta, experts, topk, cap):
    n = meta.shape[1]
    count = experts.shape[0] * cap

    def kernel(m_ref, e_ref, out):
        for i, mat in enumerate(route(m_ref[...], e_ref[...], topk, cap, True)):
            out[:, i * count : (i + 1) * count] = mat.astype(F32).T.astype(BF)

    return pl.pallas_call(
        kernel,
        out_shape=jax.ShapeDtypeStruct((n, 2 * count), BF),
        cost_estimate=cost(1e9, n * count * 4),
        compiler_params=SMALL,
        name="combine_matrix",
    )(meta, experts)


def column_piece(arrays, rows, wide, piece, pieces):
    inside = piece % (pieces // len(arrays))
    return arrays[piece * len(arrays) // pieces], pl.BlockSpec((rows, wide), lambda i: (0, inside))


def combine_piece(matrix, parts, piece, pieces):
    n = matrix.shape[0]
    rows = parts[0][0].shape[0]
    wide = sum(a.shape[1] for a in parts[0]) // pieces

    def kernel(m_ref, *refs):
        stacked = jnp.concatenate([r[...] for r in refs[:-1]], axis=0)
        count = stacked.shape[0]
        total = jnp.dot(m_ref[:, :count], stacked, preferred_element_type=F32)
        total = total + jnp.dot(m_ref[:, count:], stacked, preferred_element_type=F32)
        refs[-1][...] = total.astype(BF)

    args, specs = zip(*[column_piece(p, rows, wide, piece, pieces) for p in parts])
    return pl.pallas_call(
        kernel,
        grid=(1,),
        in_specs=[pl.BlockSpec(matrix.shape, lambda i: (0, 0))] + list(specs),
        out_specs=pl.BlockSpec((n, wide), lambda i: (0, 0)),
        out_shape=jax.ShapeDtypeStruct((n, wide), BF),
        cost_estimate=cost(1e9, n * wide * 8),
        compiler_params=SMALL,
        name="combine_piece",
    )(matrix, *args)


def expert_ffn(parts, gain, weights, splits, dtype):
    local_exp, rows, d = parts[0][0].shape
    n = len(parts)
    flat = [a for p in parts for a in p]
    count = len(flat)
    wides = [d // c for counts in splits for c in counts for _ in range(c)]
    total = len(wides)

    def kernel(*refs):
        x_in, gain_ref, w_in = refs[:count], refs[count], refs[count + 1 : count + 7]
        outs, x_s = refs[count + 7 : count + 7 + total], refs[count + 7 + total]
        for e in range(local_exp):
            at = 0
            for i, group in enumerate(parts):
                x = x_in[at][e].astype(F32)
                for more in range(1, len(group)):
                    x = x + x_in[at + more][e].astype(F32)
                at += len(group)
                scale = lax.rsqrt(jnp.mean(x * x, axis=-1, keepdims=True) + 1e-06)
                low = (e * n + i) * rows
                x_s[low : low + rows, :] = (x * scale * gain_ref[...]).astype(BF)
        for e in range(local_exp):
            x = x_s[e * n * rows : (e + 1) * n * rows, :]
            hidden = []
            for half in range(2):
                gate, up = w_in[3 * half], w_in[3 * half + 1]
                a = jnp.dot(x, gate[e], preferred_element_type=F32)
                b = jnp.dot(x, up[e], preferred_element_type=F32)
                hidden.append(((a / (1.0 + jnp.exp(-a))) * b).astype(BF))
            y = jnp.dot(hidden[0], w_in[2][e], preferred_element_type=F32)
            y = y + jnp.dot(hidden[1], w_in[5][e], preferred_element_type=F32)
            at = 0
            for i in range(n):
                for pieces in splits[i]:
                    wide = d // pieces
                    for c in range(pieces):
                        piece = y[i * rows : (i + 1) * rows, c * wide : (c + 1) * wide]
                        outs[at][e] = piece.astype(dtype)
                        at += 1

    whole = pl.BlockSpec(memory_space=pltpu.VMEM)
    return pl.pallas_call(
        kernel,
        in_specs=[whole] * (count + 7),
        out_specs=[whole] * total,
        out_shape=[jax.ShapeDtypeStruct((local_exp, rows, w), dtype) for w in wides],
        scratch_shapes=[pltpu.VMEM((local_exp * n * rows, d), BF)],
        compiler_params=LARGE,
        cost_estimate=cost(6e9, 6 * weights[0].size * 2),
        name="expert_ffn",
    )(*flat, gain, *weights)


def finish(base, lists, chunk, chunks, out):
    n, d = base.shape
    wide = d // chunks

    args, specs = zip(*[column_piece(arrays, n, wide, chunk, chunks) for arrays in [[base]] + lists])
    args, specs = list(args), list(specs)
    count = len(args)
    alias = {}
    if out is not None:
        alias = {count: 0}
        args.append(out)
        specs.append(pl.BlockSpec(memory_space=pl.ANY))

    def kernel(*refs):
        total = None
        for ref in refs[:count]:
            v = ref[...].astype(F32)
            total = v if total is None else total + v
        refs[-1][...] = total.astype(BF)

    return pl.pallas_call(
        kernel,
        grid=(1,),
        in_specs=specs,
        out_specs=pl.BlockSpec((n, wide), lambda i: (0, chunk)),
        out_shape=jax.ShapeDtypeStruct((n, d), BF),
        input_output_aliases=alias,
        cost_estimate=cost(1e9, 3e6 / chunks),
        compiler_params=SMALL,
        name="finish",
    )(*args)


def body(outer, inner, chunks, tokens, norm_gain, expert_ids, gate_values, w_gate, w_up, w_down, s_gate, s_up, s_down):
    n_rows, width = tokens.shape
    topk = expert_ids.shape[1]
    local_exp = w_gate.shape[0]
    cap = 2 * n_rows * topk // (local_exp * outer * inner)
    half = outer // 2
    me = lax.axis_index("ep")
    z, y = me // inner, me % inner

    def along(pairs):
        return [(a * inner + j, b * inner + j) for a, b in pairs for j in range(inner)]

    def send(x, pairs):
        return lax.ppermute(x, "ep", pairs)

    def across(x, k):
        return send(x, [(i, (i // inner) * inner + (i % inner ^ k)) for i in range(outer * inner)])

    def swap_core(x):
        return lax.ppermute(x, "tp", [(0, 1), (1, 0)])

    slot_block = [list(range(outer))]
    levels = []
    size = 1
    while size < half:
        level = []
        for j in range(size):
            exchange, table = [], [0] * outer
            hops = [[] for _ in range(size - 1)]
            for start in range(0, outer, 2 * size):
                left, right = start + size - 1, start + size
                exchange += [(left, right), (right, left)]
                for d in range(size):
                    table[left - d] = slot_block[j][right]
                    table[right + d] = slot_block[j][left]
                    if d:
                        hops[d - 1] += [(left - d + 1, left - d), (right + d - 1, right + d)]
            level.append((j, exchange, hops, table))
        for entry in level:
            slot_block.append(entry[3])
        levels.append(level)
        size *= 2
    edge = [half - 1 if i < half else half for i in range(outer)]
    away = [-1 if i < half else 1 for i in range(outer)]
    top_block = [[slot_block[j][half if i < half else half - 1] for i in range(outer)] for j in range(half)]
    exchange_top = [(half - 1, half), (half, half - 1)]
    outward = {}
    for d in range(half):
        for k in range(inner):
            pairs = [(edge[i], edge[i] + away[i] * d) for i in (half - 1, half)]
            outward[d, k] = [(a * inner + j, b * inner + (j ^ k)) for a, b in pairs for j in range(inner)]
    inward = {dk: [(b, a) for a, b in pairs] for dk, pairs in outward.items()}

    meta = jnp.concatenate([expert_ids.T.astype(F32), gate_values.T], axis=0)
    gain = norm_gain.reshape(1, width)

    def experts_at(positions):
        bases = [position * inner + (y ^ k) for position in positions for k in range(inner)]
        return jnp.stack([(base * local_exp + j).astype(F32) for base in bases for j in range(local_exp)]).reshape(-1, 1)

    edge_z = jnp.where(z < half, half - 1, half)
    away_z = jnp.where(z < half, -1, 1)
    here = experts_at([z])
    side = experts_at([edge_z + away_z * d for d in range(half)])

    slots, metas = [tokens], [meta]
    for level in levels:
        for j, exchange, hops, _ in level:
            s = len(slots)
            cur, cur_m = send(slots[j], along(exchange)), send(metas[j], along(exchange))
            total, total_m = cur, cur_m
            for pairs in hops:
                cur, cur_m = send(cur, along(pairs)), send(cur_m, along(pairs))
                total, total_m = total + cur, total_m + cur_m
            slots.append(total)
            metas.append(total_m)
    straight = [[(top_block[j][b], b) for b in (half - 1, half)] for j in range(half)]
    top_metas = [send(meta, along(straight[j])) for j in range(half)]
    tops = [send(slots[j], along(exchange_top)) for j in range(half)]

    s_own = [w[None] for w in (s_gate, s_up, s_down)]
    s_others = [swap_core(w)[None] for w in (s_gate, s_up, s_down)]
    routed_w = [w_gate, w_up, w_down] + [swap_core(w) for w in (w_gate, w_up, w_down)]

    def shaped(a):
        return a.reshape(local_exp, cap, width)

    def experts(sources, splits):
        outs = expert_ffn([[shaped(a) for a in part] for part in sources], gain, routed_w, splits, BF)
        outs = [a.reshape(local_exp * cap, a.shape[-1]) for a in outs]
        result, at = [], 0
        for counts in splits:
            result.append([])
            for c in counts:
                result[-1].append(outs[at : at + c])
                at += c
        return result

    shared = expert_ffn([[tokens[None]]], gain, s_own + s_others, [(1,)], F32)[0][0]

    def plus(a, b):
        return (a.astype(F32) + b.astype(F32)).astype(BF)

    sums = []
    for s, block in enumerate(slots):
        rows = compact(block, metas[s], here, topk, local_exp, cap)
        got = [across(rows[k], k) for k in range(1, inner)]
        outs = experts([[rows[0]]] + [[a] for a in got], [(1,)] * inner)
        outs = [o[0][0] for o in outs]
        parts = [outs[0]] + [across(outs[k], k) for k in range(1, inner)]
        if s == 0:
            sums.append(combine(metas[s], here, topk, parts, cap, [shared], F32, 1))
        else:
            sums.append(combine(metas[s], here, topk, parts, cap, [], BF, chunks))

    arrived = [[] for _ in slots]
    for j, block in enumerate(tops):
        rows = compact(block, top_metas[j], side, topk, local_exp, cap)
        matrix = combine_matrix(top_metas[j], side, topk, cap)
        mine = [[rows[0]]] + [[] for _ in range(1, inner)]
        for d in reversed(range(half)):
            for k in reversed(range(inner)):
                if d or k:
                    mine[k].append(send(rows[d * inner + k], outward[d, k]))
        pieces = max(1, chunks // 2) if j == 0 else chunks
        results = experts(mine, [(pieces,)] * inner)
        near = [results[0][0]]
        near += [[across(a, k) for a in results[k][0]] for k in range(1, inner)]
        far = [[send(a, inward[d, 0]) for a in part] for d in range(1, half) for part in near]
        got = []
        for c in range(pieces):
            total = combine_piece(matrix, near + far, c, pieces)
            got.append(send(total, along(exchange_top)))
        arrived[j].append(got)

    slot = len(slots)
    for level in reversed(levels):
        for j, exchange, hops, _ in reversed(level):
            slot -= 1
            late = sums[slot]
            for more in arrived[slot]:
                late = [plus(a, b) for a, b in zip(late, more)]
            for pairs in reversed(hops):
                back = [(b, a) for a, b in pairs]
                late = [plus(a, send(a, along(back))) for a in late]
            arrived[j].append([send(a, along(exchange)) for a in late])
    out = None
    for c in range(chunks):
        out = finish(sums[0][0], arrived[0], c, chunks, out)
    return out


def solution(mesh):
    ep = mesh.shape["ep"]
    bits = ep.bit_length() - 1
    outer = 1 << ((bits + 1) // 2)
    chunks = max(1, CHUNKS * 2 // (ep // outer))

    def layer(*args):
        return body(outer, ep // outer, chunks, *args)

    return jax.shard_map(
        layer,
        mesh=mesh,
        in_specs=(
            P(("grp", "ep", "tp"), None),
            P(),
            P(("grp", "ep", "tp"), None),
            P(("grp", "ep", "tp"), None),
            P("ep", None, "tp"),
            P("ep", None, "tp"),
            P("ep", "tp", None),
            P(None, "tp"),
            P(None, "tp"),
            P("tp", None),
        ),
        out_specs=P(("grp", "ep", "tp"), None),
        check_vma=False,
    )
```

time: 273 us -> 225 us (0.82)
  waiting for transfers between devices: 177 us -> 56.9 us
  starting transfers between devices: 12.4 us -> 125 us
  Pallas kernels: 0 us -> 37.8 us
  matrix products: 26.6 us -> 0 us
  local copies, waits for them, and re-layouts: 25.5 us -> 1.97 us
  other arithmetic: 17.1 us -> 1.73 us
  between operations: 13.3 us -> 0.73 us
    all_to_all x2 -> x0, waiting for transfers between devices: 175 us -> none  [the longest x1 92.2 us: body(): lax.all_to_all(results.astype(jnp.bfloat16), 'ep', split_axis=0, concat_a...]
    ppermute x0 -> x50, starting transfers between devices: none -> 125 us  [the longest x44 123 us: send(): return lax.ppermute(x, 'ep', pairs)]
    ppermute x0 -> x50, waiting for transfers between devices: none -> 56.9 us  [the longest x44 56.9 us: send(): return lax.ppermute(x, 'ep', pairs)]
    pallas_call x0 -> x23, Pallas kernels: none -> 37.8 us  [the longest x5 21.3 us: expert_ffn(): pl.pallas_call(kernel, in_specs=[whole] * (count + 7), out_specs=[whole]...]
    dot_general x4 -> x0, matrix products: 26.6 us -> none  [the longest x1 11.2 us: body(): jnp.einsum('xecf,efd->xecd', hidden, full_down, preferred_element_type=jn...]
    gather x2 -> x0, local copies, waits for them, and re-layouts: 13.2 us -> none  [the longest x1 7.13 us: body(): returned.reshape(experts_n * capacity, width)[position]]
    all_to_all x2 -> x0, starting transfers between devices: 12.2 us -> none  [the longest x1 7.31 us: body(): lax.all_to_all(outgoing, 'ep', split_axis=0, concat_axis=0, tiled=True)]
    reduce_sum x3 -> x0, other arithmetic: 10.5 us -> none  [the longest x1 8.86 us: body(): jnp.sum(gate_values[:, :, None] * picked.astype(jnp.float32), axis=1)]
  transfers between devices with their start and end apart: 7 -> 50, of which waited for: 2 -> 10; matrix products, arithmetic and copies ran while one was open for 23% -> 1% of each run, Pallas kernels for 0% -> 17%
where the time goes in v1:
time: 225 us; the launch traced here: 224 us
  starting transfers between devices  125 us (56%)
  waiting for transfers between devices  56.9 us (25%)
  Pallas kernels  37.8 us (17%)
    ppermute x44, starting transfers between devices, send(): return lax.ppermute(x, 'ep', pairs)  123 us
    ppermute x44, waiting for transfers between devices, send(): return lax.ppermute(x, 'ep', pairs)  56.9 us
    pallas_call x5, Pallas kernels, expert_ffn(): pl.pallas_call(kernel, in_specs=[whole] * (count + 7), out_specs=[whole]...  21.3 us
    pallas_call x4, Pallas kernels, compact(): pl.pallas_call(kernel, grid=(steps,), in_specs=[pl.BlockSpec((n, wide), l...  7.46 us
  transfers between devices with their start and end apart: 50, of which 10 were waited for; matrix products, arithmetic and copies ran while one was open for 1% of the time, Pallas kernels for 17%

profile of v1, /device:TPU:0, one launch (start us, length us, event | category | flops | bytes accessed | tf_op | source)
XLA Modules:
  0.0 224.1 jit_solution(17742985967177268906)
XLA Ops:
  2.2 4.5 %collective-permute-start.18 = (bf16[256,2048]{1,0:T(8,128)(2,1)}, bf16[256,2048]{1,0:T(8,128)(2,1)}, u32[]{:S(2)}, u32[]{:S(2)}) collective-permute-start(bf16[256,2048]{1,0:T(8,128)(2,1)} %x_ref.1), channel_id=1, source_target_pairs={{0,4},{2,6},{4,0},{6,2},{8,12},{10,14},{12,8},{14,10},{1,5},{3,7},... | collective-permute-start | bytes 3145736 | tf_op jit(solution)/shard_map/ppermute | solution.py:253
  8.1 2.5 %collective-permute-start.21 = (f32[4,256]{1,0:T(4,128)S(1)}, f32[4,256]{1,0:T(4,128)S(1)}, u32[]{:S(2)}, u32[]{:S(2)}) collective-permute-start(f32[4,256]{1,0:T(4,128)S(1)} %pad_maximum_fusion.m_ref), channel_id=1, source_target_pairs={{12,4},{14,6},{0,8},{2,10},{13,5},{15,7},{1,9},{3,11},{28,20},{30,... | collective-permute-start | bytes 12296 | tf_op jit(solution)/shard_map/ppermute | solution.py:253
  11.2 18.8 %collective-permute-done.21.m_ref = f32[4,256]{1,0:T(4,128)S(1)} collective-permute-done((f32[4,256]{1,0:T(4,128)S(1)}, f32[4,256]{1,0:T(4,128)S(1)}, u32[]{:S(2)}, u32[]{:S(2)}) %collective-permute-start.21) | collective-permute-done | bytes 4128 | tf_op jit(solution)/shard_map/ppermute | solution.py:253
  30.7 2.3 %collective-permute-start.17 = (f32[4,256]{1,0:T(4,128)S(1)}, f32[4,256]{1,0:T(4,128)S(1)}, u32[]{:S(2)}, u32[]{:S(2)}) collective-permute-start(f32[4,256]{1,0:T(4,128)S(1)} %pad_maximum_fusion.m_ref), channel_id=1, source_target_pairs={{0,4},{2,6},{4,0},{6,2},{8,12},{10,14},{12,8},{14,10},{1,5},{3,7},... | collective-permute-start | bytes 12296 | tf_op jit(solution)/shard_map/ppermute | solution.py:253
  33.1 3.0 %compact_rows.5 = (bf16[128,2048]{1,0:T(8,128)(2,1)S(1)}, bf16[128,2048]{1,0:T(8,128)(2,1)}, bf16[128,2048]{1,0:T(8,128)(2,1)S(1)}, bf16[128,2048]{1,0:T(8,128)(2,1)}) custom-call(bf16[256,2048]{1,0:T(8,128)(2,1)} %collective-permute-done.9.x_ref, f32[4,256]{1,0:T(4,128)S(1)} %collective-permute-done.8.m_ref, f32[8,1]{1,0:T(8,128)S(1)} %copy.16.e_ref), custom_call_target="tpu_custom_call" | custom-call | flops 2000000000 | bytes 2097152 | tf_op jit(solution)/shard_map/compact_rows/pallas_call | solution.py:61
  39.5 14.1 %collective-permute-done.10 = bf16[128,2048]{1,0:T(8,128)(2,1)S(1)} collective-permute-done((bf16[128,2048]{1,0:T(8,128)(2,1)S(1)}, bf16[128,2048]{1,0:T(8,128)(2,1)S(1)}, u32[]{:S(2)}, u32[]{:S(2)}) %collective-permute-start.10) | collective-permute-done | bytes 524320 | tf_op jit(solution)/shard_map/ppermute | solution.py:253
  56.1 8.5 %collective-permute-done.11 = bf16[128,2048]{1,0:T(8,128)(2,1)} collective-permute-done((bf16[128,2048]{1,0:T(8,128)(2,1)}, bf16[128,2048]{1,0:T(8,128)(2,1)}, u32[]{:S(2)}, u32[]{:S(2)}) %collective-permute-start.11) | collective-permute-done | bytes 524320 | tf_op jit(solution)/shard_map/ppermute | solution.py:253
  67.1 2.1 compact_rows.6
  70.6 5.2 %expert_ffn.7 = (bf16[2,64,1024]{2,1,0:T(8,128)(2,1)S(1)}, bf16[2,64,1024]{2,1,0:T(8,128)(2,1)S(1)}, bf16[2,64,1024]{2,1,0:T(8,128)(2,1)S(1)}, bf16[2,64,1024]{2,1,0:T(8,128)(2,1)S(1)}) custom-call(bf16[2,64,2048]{2,1,0:T(8,128)(2,1)S(1)} %bitcast.98, bf16[2,64,2048]{2,1,0:T(8,128)(2,1)S(1)} %bitcast.65, bf16[2,64,2048]{2,1,0:T(8,128)(2,1)} %bitcast.31.refs_2_, ...), custom_call_target="tpu_custom_call" | custom-call | flops 6000000000 | bytes 12582912 | tf_op jit(solution)/shard_map/expert_ffn/pallas_call | solution.py:195
  78.0 2.2 expert_ffn.6
  82.8 22.4 %collective-permute-start.37 = (bf16[128,1024]{1,0:T(8,128)(2,1)S(1)}, bf16[128,1024]{1,0:T(8,128)(2,1)S(1)}, u32[]{:S(2)}, u32[]{:S(2)}) collective-permute-start(bf16[128,1024]{1,0:T(8,128)(2,1)S(1)} %bitcast.72), channel_id=1, source_target_pairs={{0,4},{2,6},{12,8},{14,10},{1,5},{3,7},{13,9},{15,11},{16,20},{18,... | collective-permute-start | bytes 786440 | tf_op jit(solution)/shard_map/ppermute | solution.py:253
  107.2 4.6 %expert_ffn.8 = (bf16[2,64,2048]{2,1,0:T(8,128)(2,1)S(1)}, bf16[2,64,2048]{2,1,0:T(8,128)(2,1)S(1)}) custom-call(bf16[2,64,2048]{2,1,0:T(8,128)(2,1)S(1)} %bitcast.99, bf16[2,64,2048]{2,1,0:T(8,128)(2,1)S(1)} %bitcast.69, f32[1,2048]{1,0:T(1,128)S(1)} %bitcast.90, bf16[2,2048,256]{2,1,0:T(8,128)(2,1)S(1)} %copy-done, bf16[2,2048,256]{2,1,0:T(8,128)(2,1)S(1)} %copy-done.1, ...), custom_call_target="tpu_custom_call" | custom-call | flops 6000000000 | bytes 12582912 | tf_op jit(solution)/shard_map/expert_ffn/pallas_call | solution.py:195
  113.8 7.3 %collective-permute-start.14 = (bf16[128,1024]{1,0:T(8,128)(2,1)S(1)}, bf16[128,1024]{1,0:T(8,128)(2,1)S(1)}, u32[]{:S(2)}, u32[]{:S(2)}) collective-permute-start(bf16[128,1024]{1,0:T(8,128)(2,1)S(1)} %bitcast.70), channel_id=1, source_target_pairs={{0,4},{2,6},{12,8},{14,10},{1,5},{3,7},{13,9},{15,11},{16,20},{18,... | collective-permute-start | bytes 786440 | tf_op jit(solution)/shard_map/ppermute | solution.py:253
  122.6 4.6 %expert_ffn.5 = (bf16[2,64,2048]{2,1,0:T(8,128)(2,1)S(1)}, bf16[2,64,2048]{2,1,0:T(8,128)(2,1)S(1)}) custom-call(bf16[2,64,2048]{2,1,0:T(8,128)(2,1)S(1)} %bitcast.94, bf16[2,64,2048]{2,1,0:T(8,128)(2,1)S(1)} %bitcast.62, f32[1,2048]{1,0:T(1,128)S(1)} %bitcast.91, bf16[2,2048,256]{2,1,0:T(8,128)(2,1)S(1)} %copy-done, bf16[2,2048,256]{2,1,0:T(8,128)(2,1)S(1)} %copy-done.1, ...), custom_call_target="tpu_custom_call" | custom-call | flops 6000000000 | bytes 12582912 | tf_op jit(solution)/shard_map/expert_ffn/pallas_call | solution.py:195
  132.3 4.7 %expert_ffn.9 = (bf16[2,64,512]{2,1,0:T(8,128)(2,1)S(1)}, bf16[2,64,512]{2,1,0:T(8,128)(2,1)S(1)}, bf16[2,64,512]{2,1,0:T(8,128)(2,1)S(1)}, bf16[2,64,512]{2,1,0...) custom-call(bf16[2,64,2048]{2,1,0:T(8,128)(2,1)S(1)} %bitcast.96, ...), custom_call_target="tpu_custom_call" | custom-call | flops 6000000000 | bytes 12582912 | tf_op jit(solution)/shard_map/expert_ffn/pallas_call | solution.py:195
  137.9 4.4 %collective-permute-start.46 = (bf16[128,512]{1,0:T(8,128)(2,1)S(1)}, bf16[128,512]{1,0:T(8,128)(2,1)S(1)}, u32[]{:S(2)}, u32[]{:S(2)}) collective-permute-start(bf16[128,512]{1,0:T(8,128)(2,1)S(1)} %bitcast.83), channel_id=1, source_target_pairs={{0,4},{2,6},{12,8},{14,10},{1,5},{3,7},{13,9},{15,11},{16,20},{18,... | collective-permute-start | bytes 393224 | tf_op jit(solution)/shard_map/ppermute | solution.py:253
  143.6 3.1 %collective-permute-start.41 = (bf16[128,512]{1,0:T(8,128)(2,1)S(1)}, bf16[128,512]{1,0:T(8,128)(2,1)S(1)}, u32[]{:S(2)}, u32[]{:S(2)}) collective-permute-start(bf16[128,512]{1,0:T(8,128)(2,1)S(1)} %bitcast.80), channel_id=1, source_target_pairs={{0,4},{2,6},{12,8},{14,10},{1,5},{3,7},{13,9},{15,11},{16,20},{18,... | collective-permute-start | bytes 393224 | tf_op jit(solution)/shard_map/ppermute | solution.py:253
  147.6 6.4 %collective-permute-done.4.refs_1_ = bf16[128,2048]{1,0:T(8,128)(2,1)S(1)} collective-permute-done((bf16[128,2048]{1,0:T(8,128)(2,1)S(1)}, bf16[128,2048]{1,0:T(8,128)(2,1)S(1)}, u32[]{:S(2)}, u32[]{:S(2)}) %collective-permute-start.4) | collective-permute-done | bytes 524320 | tf_op jit(solution)/shard_map/ppermute | solution.py:253
  158.2 3.8 %collective-permute-start.47 = (bf16[128,512]{1,0:T(8,128)(2,1)S(1)}, bf16[128,512]{1,0:T(8,128)(2,1)S(1)}, u32[]{:S(2)}, u32[]{:S(2)}) collective-permute-start(bf16[128,512]{1,0:T(8,128)(2,1)S(1)} %collective-permute-done.45.refs_1_), channel_id=1, source_target_pairs={{0,4},{2,6},{12,8},{14,10},{1,5},{3,7},{13,9},{15,11},{16,20},{18,... | collective-permute-start | bytes 393224 | tf_op jit(solution)/shard_map/ppermute | solution.py:253
  165.6 4.4 %collective-permute-start.33 = (bf16[128,512]{1,0:T(8,128)(2,1)S(1)}, bf16[128,512]{1,0:T(8,128)(2,1)S(1)}, u32[]{:S(2)}, u32[]{:S(2)}) collective-permute-start(bf16[128,512]{1,0:T(8,128)(2,1)S(1)} %collective-permute-done.31.refs_1_), channel_id=1, source_target_pairs={{0,4},{2,6},{12,8},{14,10},{1,5},{3,7},{13,9},{15,11},{16,20},{18,... | collective-permute-start | bytes 393224 | tf_op jit(solution)/shard_map/ppermute | solution.py:253
  178.7 29.8 %collective-permute-start.49 = (bf16[256,512]{1,0:T(8,128)(2,1)S(1)}, bf16[256,512]{1,0:T(8,128)(2,1)S(1)}, u32[]{:S(2)}, u32[]{:S(2)}) collective-permute-start(bf16[256,512]{1,0:T(8,128)(2,1)S(1)} %add_convert_fusion), channel_id=1, source_target_pairs={{0,4},{2,6},{4,0},{6,2},{8,12},{10,14},{12,8},{14,10},{1,5},{3,7},... | collective-permute-start | bytes 786440 | tf_op jit(solution)/shard_map/ppermute | solution.py:253
  208.6 2.7 %collective-permute-start.44 = (bf16[256,512]{1,0:T(8,128)(2,1)S(1)}, bf16[256,512]{1,0:T(8,128)(2,1)S(1)}, u32[]{:S(2)}, u32[]{:S(2)}) collective-permute-start(bf16[256,512]{1,0:T(8,128)(2,1)S(1)} %add_convert_fusion.1), channel_id=1, source_target_pairs={{0,4},{2,6},{4,0},{6,2},{8,12},{10,14},{12,8},{14,10},{1,5},{3,7},... | collective-permute-start | bytes 786440 | tf_op jit(solution)/shard_map/ppermute | solution.py:253
  211.4 2.7 %collective-permute-start.35 = (bf16[256,512]{1,0:T(8,128)(2,1)S(1)}, bf16[256,512]{1,0:T(8,128)(2,1)S(1)}, u32[]{:S(2)}, u32[]{:S(2)}) collective-permute-start(bf16[256,512]{1,0:T(8,128)(2,1)S(1)} %add_convert_fusion.2), channel_id=1, source_target_pairs={{0,4},{2,6},{4,0},{6,2},{8,12},{10,14},{12,8},{14,10},{1,5},{3,7},... | collective-permute-start | bytes 786440 | tf_op jit(solution)/shard_map/ppermute | solution.py:253
  218.5 2.0 collective-permute-done.35.refs_2_
  (133 shorter events, 57.3 us)
Async XLA Ops:
  0.0 30.7 %collective-permute-start.9 = (bf16[256,2048]{1,0:T(8,128)(2,1)}, bf16[256,2048]{1,0:T(8,128)(2,1)}, u32[]{:S(2)}, u32[]{:S(2)}) collective-permute-start(bf16[256,2048]{1,0:T(8,128)(2,1)} %x_ref.1), channel_id=1, source_target_pairs={{4,8},{6,10},{8,4},{10,6},{5,9},{7,11},{9,5},{11,7},{20,24},{22,26... | collective-permute-start | bytes 3145736 | tf_op jit(solution)/shard_map/ppermute | solution.py:253
  1.7 63.5 %collective-permute-start.1 = (bf16[2,2048,256]{2,1,0:T(8,128)(2,1)}, bf16[2,2048,256]{2,1,0:T(8,128)(2,1)S(1)}, u32[]{:S(2)}, u32[]{:S(2)}) collective-permute-start(bf16[2,2048,256]{2,1,0:T(8,128)(2,1)} %refs_5_.7), channel_id=1, source_target_pairs={{0,1},{1,0},{2,3},{3,2},{4,5},{5,4},{6,7},{7,6},{8,9},{9,8},{10,11... | collective-permute-start | bytes 6291464 | tf_op jit(solution)/shard_map/ppermute | solution.py:259
  2.2 36.0 %collective-permute-start.18 = (bf16[256,2048]{1,0:T(8,128)(2,1)}, bf16[256,2048]{1,0:T(8,128)(2,1)}, u32[]{:S(2)}, u32[]{:S(2)}) collective-permute-start(bf16[256,2048]{1,0:T(8,128)(2,1)} %x_ref.1), channel_id=1, source_target_pairs={{0,4},{2,6},{4,0},{6,2},{8,12},{10,14},{12,8},{14,10},{1,5},{3,7},... | collective-permute-start | bytes 3145736 | tf_op jit(solution)/shard_map/ppermute | solution.py:253
  8.1 22.0 %collective-permute-start.21 = (f32[4,256]{1,0:T(4,128)S(1)}, f32[4,256]{1,0:T(4,128)S(1)}, u32[]{:S(2)}, u32[]{:S(2)}) collective-permute-start(f32[4,256]{1,0:T(4,128)S(1)} %pad_maximum_fusion.m_ref), channel_id=1, source_target_pairs={{12,4},{14,6},{0,8},{2,10},{13,5},{15,7},{1,9},{3,11},{28,20},{30,... | collective-permute-start | bytes 12296 | tf_op jit(solution)/shard_map/ppermute | solution.py:253
  10.6 19.5 %collective-permute-start.8 = (f32[4,256]{1,0:T(4,128)S(1)}, f32[4,256]{1,0:T(4,128)S(1)}, u32[]{:S(2)}, u32[]{:S(2)}) collective-permute-start(f32[4,256]{1,0:T(4,128)S(1)} %pad_maximum_fusion.m_ref), channel_id=1, source_target_pairs={{8,4},{10,6},{4,8},{6,10},{9,5},{11,7},{5,9},{7,11},{24,20},{26,22... | collective-permute-start | bytes 12296 | tf_op jit(solution)/shard_map/ppermute | solution.py:253
  30.1 39.1 %collective-permute-start.2 = (bf16[2,2048,256]{2,1,0:T(8,128)(2,1)}, bf16[2,2048,256]{2,1,0:T(8,128)(2,1)}, u32[]{:S(2)}, u32[]{:S(2)}) collective-permute-start(bf16[2,2048,256]{2,1,0:T(8,128)(2,1)} %refs_6_.3), channel_id=1, source_target_pairs={{0,1},{1,0},{2,3},{3,2},{4,5},{5,4},{6,7},{7,6},{8,9},{9,8},{10,11... | collective-permute-start | bytes 6291464 | tf_op jit(solution)/shard_map/ppermute | solution.py:259
  30.1 39.7 %collective-permute-start.3 = (bf16[2,256,2048]{2,1,0:T(8,128)(2,1)}, bf16[2,256,2048]{2,1,0:T(8,128)(2,1)}, u32[]{:S(2)}, u32[]{:S(2)}) collective-permute-start(bf16[2,256,2048]{2,1,0:T(8,128)(2,1)} %refs_7_.3), channel_id=1, source_target_pairs={{0,1},{1,0},{2,3},{3,2},{4,5},{5,4},{6,7},{7,6},{8,9},{9,8},{10,11... | collective-permute-start | bytes 6291464 | tf_op jit(solution)/shard_map/ppermute | solution.py:259
  38.2 26.4 %collective-permute-start.11 = (bf16[128,2048]{1,0:T(8,128)(2,1)}, bf16[128,2048]{1,0:T(8,128)(2,1)}, u32[]{:S(2)}, u32[]{:S(2)}) collective-permute-start(bf16[128,2048]{1,0:T(8,128)(2,1)} %get-tuple-element.43), channel_id=1, source_target_pairs={{4,2},{6,0},{8,14},{10,12},{5,3},{7,1},{9,15},{11,13},{20,18},{22,... | collective-permute-start | bytes 1572872 | tf_op jit(solution)/shard_map/ppermute | solution.py:253
  69.2 42.6 %collective-permute-start = (bf16[128,2048]{1,0:T(8,128)(2,1)S(1)}, bf16[128,2048]{1,0:T(8,128)(2,1)S(1)}, u32[]{:S(2)}, u32[]{:S(2)}) collective-permute-start(bf16[128,2048]{1,0:T(8,128)(2,1)S(1)} %get-tuple-element.38), channel_id=1, source_target_pairs={{0,2},{2,0},{4,6},{6,4},{8,10},{10,8},{12,14},{14,12},{1,3},{3,1},... | collective-permute-start | bytes 1572872 | tf_op jit(solution)/shard_map/ppermute | solution.py:253
  75.8 29.4 %collective-permute-start.19 = (bf16[128,2048]{1,0:T(8,128)(2,1)S(1)}, bf16[128,2048]{1,0:T(8,128)(2,1)S(1)}, u32[]{:S(2)}, u32[]{:S(2)}) collective-permute-start(bf16[128,2048]{1,0:T(8,128)(2,1)S(1)} %get-tuple-element.48), channel_id=1, source_target_pairs={{0,2},{2,0},{4,6},{6,4},{8,10},{10,8},{12,14},{14,12},{1,3},{3,1},... | collective-permute-start | bytes 1572872 | tf_op jit(solution)/shard_map/ppermute | solution.py:253
  77.4 28.5 %collective-permute-start.36 = (bf16[128,1024]{1,0:T(8,128)(2,1)S(1)}, bf16[128,1024]{1,0:T(8,128)(2,1)S(1)}, u32[]{:S(2)}, u32[]{:S(2)}) collective-permute-start(bf16[128,1024]{1,0:T(8,128)(2,1)S(1)} %bitcast.75), channel_id=1, source_target_pairs={{0,2},{2,0},{4,6},{6,4},{8,10},{10,8},{12,14},{14,12},{1,3},{3,1},... | collective-permute-start | bytes 786440 | tf_op jit(solution)/shard_map/ppermute | solution.py:253
  81.5 50.8 %collective-permute-start.23 = (bf16[128,2048]{1,0:T(8,128)(2,1)S(1)}, bf16[128,2048]{1,0:T(8,128)(2,1)S(1)}, u32[]{:S(2)}, u32[]{:S(2)}) collective-permute-start(bf16[128,2048]{1,0:T(8,128)(2,1)S(1)} %get-tuple-element.53), channel_id=1, source_target_pairs={{4,0},{6,2},{8,12},{10,14},{5,1},{7,3},{9,13},{11,15},{20,16},{22,... | collective-permute-start | bytes 1572872 | tf_op jit(solution)/shard_map/ppermute | solution.py:253
  82.8 30.3 %collective-permute-start.37 = (bf16[128,1024]{1,0:T(8,128)(2,1)S(1)}, bf16[128,1024]{1,0:T(8,128)(2,1)S(1)}, u32[]{:S(2)}, u32[]{:S(2)}) collective-permute-start(bf16[128,1024]{1,0:T(8,128)(2,1)S(1)} %bitcast.72), channel_id=1, source_target_pairs={{0,4},{2,6},{12,8},{14,10},{1,5},{3,7},{13,9},{15,11},{16,20},{18,... | collective-permute-start | bytes 786440 | tf_op jit(solution)/shard_map/ppermute | solution.py:253
  111.8 20.5 %collective-permute-start.24 = (bf16[128,2048]{1,0:T(8,128)(2,1)S(1)}, bf16[128,2048]{1,0:T(8,128)(2,1)S(1)}, u32[]{:S(2)}, u32[]{:S(2)}) collective-permute-start(bf16[128,2048]{1,0:T(8,128)(2,1)S(1)} %get-tuple-element.54), channel_id=1, source_target_pairs={{4,2},{6,0},{8,14},{10,12},{5,3},{7,1},{9,15},{11,13},{20,18},{22,... | collective-permute-start | bytes 1572872 | tf_op jit(solution)/shard_map/ppermute | solution.py:253
  130.3 23.7 %collective-permute-start.4 = (bf16[128,2048]{1,0:T(8,128)(2,1)S(1)}, bf16[128,2048]{1,0:T(8,128)(2,1)S(1)}, u32[]{:S(2)}, u32[]{:S(2)}) collective-permute-start(bf16[128,2048]{1,0:T(8,128)(2,1)S(1)} %bitcast.66), channel_id=1, source_target_pairs={{0,2},{2,0},{4,6},{6,4},{8,10},{10,8},{12,14},{14,12},{1,3},{3,1},... | collective-permute-start | bytes 1572872 | tf_op jit(solution)/shard_map/ppermute | solution.py:253
  137.1 19.8 %collective-permute-start.45 = (bf16[128,512]{1,0:T(8,128)(2,1)S(1)}, bf16[128,512]{1,0:T(8,128)(2,1)S(1)}, u32[]{:S(2)}, u32[]{:S(2)}) collective-permute-start(bf16[128,512]{1,0:T(8,128)(2,1)S(1)} %bitcast.87), channel_id=1, source_target_pairs={{0,2},{2,0},{4,6},{6,4},{8,10},{10,8},{12,14},{14,12},{1,3},{3,1},... | collective-permute-start | bytes 393224 | tf_op jit(solution)/shard_map/ppermute | solution.py:253
  137.9 20.3 %collective-permute-start.46 = (bf16[128,512]{1,0:T(8,128)(2,1)S(1)}, bf16[128,512]{1,0:T(8,128)(2,1)S(1)}, u32[]{:S(2)}, u32[]{:S(2)}) collective-permute-start(bf16[128,512]{1,0:T(8,128)(2,1)S(1)} %bitcast.83), channel_id=1, source_target_pairs={{0,4},{2,6},{12,8},{14,10},{1,5},{3,7},{13,9},{15,11},{16,20},{18,... | collective-permute-start | bytes 393224 | tf_op jit(solution)/shard_map/ppermute | solution.py:253
  142.3 19.7 %collective-permute-start.40 = (bf16[128,512]{1,0:T(8,128)(2,1)S(1)}, bf16[128,512]{1,0:T(8,128)(2,1)S(1)}, u32[]{:S(2)}, u32[]{:S(2)}) collective-permute-start(bf16[128,512]{1,0:T(8,128)(2,1)S(1)} %bitcast.86), channel_id=1, source_target_pairs={{0,2},{2,0},{4,6},{6,4},{8,10},{10,8},{12,14},{14,12},{1,3},{3,1},... | collective-permute-start | bytes 393224 | tf_op jit(solution)/shard_map/ppermute | solution.py:253
  143.6 26.8 %collective-permute-start.41 = (bf16[128,512]{1,0:T(8,128)(2,1)S(1)}, bf16[128,512]{1,0:T(8,128)(2,1)S(1)}, u32[]{:S(2)}, u32[]{:S(2)}) collective-permute-start(bf16[128,512]{1,0:T(8,128)(2,1)S(1)} %bitcast.80), channel_id=1, source_target_pairs={{0,4},{2,6},{12,8},{14,10},{1,5},{3,7},{13,9},{15,11},{16,20},{18,... | collective-permute-start | bytes 393224 | tf_op jit(solution)/shard_map/ppermute | solution.py:253
  174.2 40.0 %collective-permute-start.39 = (bf16[256,1024]{1,0:T(8,128)(2,1)S(1)}, bf16[256,1024]{1,0:T(8,128)(2,1)S(1)}, u32[]{:S(2)}, u32[]{:S(2)}) collective-permute-start(bf16[256,1024]{1,0:T(8,128)(2,1)S(1)} %combine_piece.9), channel_id=1, source_target_pairs={{4,8},{6,10},{8,4},{10,6},{5,9},{7,11},{9,5},{11,7},{20,24},{22,26... | collective-permute-start | bytes 1572872 | tf_op jit(solution)/shard_map/ppermute | solution.py:253
  174.9 43.5 %collective-permute-start.16 = (bf16[256,1024]{1,0:T(8,128)(2,1)S(1)}, bf16[256,1024]{1,0:T(8,128)(2,1)S(1)}, u32[]{:S(2)}, u32[]{:S(2)}) collective-permute-start(bf16[256,1024]{1,0:T(8,128)(2,1)S(1)} %combine_piece.6), channel_id=1, source_target_pairs={{4,8},{6,10},{8,4},{10,6},{5,9},{7,11},{9,5},{11,7},{20,24},{22,26... | collective-permute-start | bytes 1572872 | tf_op jit(solution)/shard_map/ppermute | solution.py:253
  176.8 31.8 %collective-permute-start.34 = (bf16[256,512]{1,0:T(8,128)(2,1)S(1)}, bf16[256,512]{1,0:T(8,128)(2,1)S(1)}, u32[]{:S(2)}, u32[]{:S(2)}) collective-permute-start(bf16[256,512]{1,0:T(8,128)(2,1)S(1)} %combine_piece.8), channel_id=1, source_target_pairs={{4,8},{6,10},{8,4},{10,6},{5,9},{7,11},{9,5},{11,7},{20,24},{22,26... | collective-permute-start | bytes 786440 | tf_op jit(solution)/shard_map/ppermute | solution.py:253
  177.9 33.5 %collective-permute-start.29 = (bf16[256,512]{1,0:T(8,128)(2,1)S(1)}, bf16[256,512]{1,0:T(8,128)(2,1)S(1)}, u32[]{:S(2)}, u32[]{:S(2)}) collective-permute-start(bf16[256,512]{1,0:T(8,128)(2,1)S(1)} %combine_piece.7), channel_id=1, source_target_pairs={{4,8},{6,10},{8,4},{10,6},{5,9},{7,11},{9,5},{11,7},{20,24},{22,26... | collective-permute-start | bytes 786440 | tf_op jit(solution)/shard_map/ppermute | solution.py:253
  178.7 36.2 %collective-permute-start.49 = (bf16[256,512]{1,0:T(8,128)(2,1)S(1)}, bf16[256,512]{1,0:T(8,128)(2,1)S(1)}, u32[]{:S(2)}, u32[]{:S(2)}) collective-permute-start(bf16[256,512]{1,0:T(8,128)(2,1)S(1)} %add_convert_fusion), channel_id=1, source_target_pairs={{0,4},{2,6},{4,0},{6,2},{8,12},{10,14},{12,8},{14,10},{1,5},{3,7},... | collective-permute-start | bytes 786440 | tf_op jit(solution)/shard_map/ppermute | solution.py:253
  (38 other events, 349.4 us)

commit v2 on v1

--- a/solution.py
+++ b/solution.py
@@ -362,10 +362,20 @@
                 if d or k:
                     mine[k].append(send(rows[d * inner + k], outward[d, k]))
         pieces = max(1, chunks // 2) if j == 0 else chunks
-        results = experts(mine, [(pieces,)] * inner)
-        near = [results[0][0]]
-        near += [[across(a, k) for a in results[k][0]] for k in range(1, inner)]
-        far = [[send(a, inward[d, 0]) for a in part] for d in range(1, half) for part in near]
+        halves = min(pieces, 2)
+        results = experts(mine, [(halves,)] * inner)
+
+        def row(arrays, d, k):
+            ends = [edge[i] + away[i] * d for i in (half - 1, half)]
+            pairs = [(e * inner + i, e * inner + (i ^ k)) for e in ends for i in range(inner)]
+            return [send(a, pairs) for a in arrays]
+
+        near = [results[0][0]] + [row(results[k][0], 0, k) for k in range(1, inner)]
+        far = []
+        for d in range(1, half):
+            crossed = [results[0][0]] + [row(results[k][0], d, k) for k in range(1, inner)]
+            for part in crossed:
+                far.append([send(a, inward[d, 0]) for a in part])
         got = []
         for c in range(pieces):
             total = combine_piece(matrix, near + far, c, pieces)

time: 225 us -> 249 us (1.11)
  waiting for transfers between devices: 56.9 us -> 120 us
  starting transfers between devices: 125 us -> 86.7 us
    ppermute x44 -> x42, waiting for transfers between devices: 56.9 us -> 120 us  [send(): return lax.ppermute(x, 'ep', pairs)]
    ppermute x44 -> x42, starting transfers between devices: 123 us -> 86.1 us  [send(): return lax.ppermute(x, 'ep', pairs)]
  transfers between devices with their start and end apart: 50 -> 48, of which waited for: 10 -> 16; matrix products, arithmetic and copies ran while one was open for 1% -> 1% of each run, Pallas kernels for 17% -> 15%
where the time goes in v2:
time: 249 us; the launch traced here: 248 us
  waiting for transfers between devices  120 us (48%)
  starting transfers between devices  86.7 us (35%)
  Pallas kernels  37 us (15%)
    ppermute x42, waiting for transfers between devices, send(): return lax.ppermute(x, 'ep', pairs)  120 us
    ppermute x42, starting transfers between devices, send(): return lax.ppermute(x, 'ep', pairs)  86.1 us
    pallas_call x5, Pallas kernels, expert_ffn(): pl.pallas_call(kernel, in_specs=[whole] * (count + 7), out_specs=[whole]...  21.2 us
    pallas_call x4, Pallas kernels, compact(): pl.pallas_call(kernel, grid=(steps,), in_specs=[pl.BlockSpec((n, wide), l...  6.86 us
  transfers between devices with their start and end apart: 48, of which 16 were waited for; matrix products, arithmetic and copies ran while one was open for 1% of the time, Pallas kernels for 15%

profile of v2, /device:TPU:0, one launch (start us, length us, event | category | flops | bytes accessed | tf_op | source)
XLA Modules:
  0.0 248.1 jit_solution(4717818235374724424)
XLA Ops:
  0.0 3.1 %collective-permute-start.19 = (bf16[256,2048]{1,0:T(8,128)(2,1)}, bf16[256,2048]{1,0:T(8,128)(2,1)S(1)}, u32[]{:S(2)}, u32[]{:S(2)}) collective-permute-start(bf16[256,2048]{1,0:T(8,128)(2,1)} %x_ref.1), channel_id=1, source_target_pairs={{0,4},{2,6},{4,0},{6,2},{8,12},{10,14},{12,8},{14,10},{1,5},{3,7},... | collective-permute-start | bytes 3145736 | tf_op jit(solution)/shard_map/ppermute | solution.py:253
  4.9 4.5 %collective-permute-start.22 = (f32[4,256]{1,0:T(4,128)S(1)}, f32[4,256]{1,0:T(4,128)S(1)}, u32[]{:S(2)}, u32[]{:S(2)}) collective-permute-start(f32[4,256]{1,0:T(4,128)S(1)} %pad_maximum_fusion.m_ref), channel_id=1, source_target_pairs={{12,4},{14,6},{0,8},{2,10},{13,5},{15,7},{1,9},{3,11},{28,20},{30,... | collective-permute-start | bytes 12296 | tf_op jit(solution)/shard_map/ppermute | solution.py:253
  9.4 16.4 %collective-permute-done.22.m_ref = f32[4,256]{1,0:T(4,128)S(1)} collective-permute-done((f32[4,256]{1,0:T(4,128)S(1)}, f32[4,256]{1,0:T(4,128)S(1)}, u32[]{:S(2)}, u32[]{:S(2)}) %collective-permute-start.22) | collective-permute-done | bytes 4128 | tf_op jit(solution)/shard_map/ppermute | solution.py:253
  25.8 3.4 %collective-permute-start.18 = (f32[4,256]{1,0:T(4,128)S(1)}, f32[4,256]{1,0:T(4,128)S(1)}, u32[]{:S(2)}, u32[]{:S(2)}) collective-permute-start(f32[4,256]{1,0:T(4,128)S(1)} %pad_maximum_fusion.m_ref), channel_id=1, source_target_pairs={{0,4},{2,6},{4,0},{6,2},{8,12},{10,14},{12,8},{14,10},{1,5},{3,7},... | collective-permute-start | bytes 12296 | tf_op jit(solution)/shard_map/ppermute | solution.py:253
  45.9 4.2 %collective-permute-done.20 = bf16[128,2048]{1,0:T(8,128)(2,1)S(1)} collective-permute-done((bf16[128,2048]{1,0:T(8,128)(2,1)S(1)}, bf16[128,2048]{1,0:T(8,128)(2,1)S(1)}, u32[]{:S(2)}, u32[]{:S(2)}) %collective-permute-start.20) | collective-permute-done | bytes 524320 | tf_op jit(solution)/shard_map/ppermute | solution.py:253
  53.5 4.7 %expert_ffn.8 = (bf16[2,64,2048]{2,1,0:T(8,128)(2,1)S(1)}, bf16[2,64,2048]{2,1,0:T(8,128)(2,1)S(1)}) custom-call(bf16[2,64,2048]{2,1,0:T(8,128)(2,1)S(1)} %bitcast.97, bf16[2,64,2048]{2,1,0:T(8,128)(2,1)S(1)} %bitcast.63, f32[1,2048]{1,0:T(1,128)S(1)} %bitcast.86, bf16[2,2048,256]{2,1,0:T(8,128)(2,1)S(1)} %copy-done, bf16[2,2048,256]{2,1,0:T(8,128)(2,1)S(1)} %copy-done.1, ...), custom_call_target="tpu_custom_call" | custom-call | flops 6000000000 | bytes 12582912 | tf_op jit(solution)/shard_map/expert_ffn/pallas_call | solution.py:195
  58.2 43.2 %collective-permute-done.10 = bf16[128,2048]{1,0:T(8,128)(2,1)S(1)} collective-permute-done((bf16[128,2048]{1,0:T(8,128)(2,1)S(1)}, bf16[128,2048]{1,0:T(8,128)(2,1)S(1)}, u32[]{:S(2)}, u32[]{:S(2)}) %collective-permute-start.10) | collective-permute-done | bytes 524320 | tf_op jit(solution)/shard_map/ppermute | solution.py:253
  103.0 10.1 %collective-permute-done.11 = bf16[128,2048]{1,0:T(8,128)(2,1)S(1)} collective-permute-done((bf16[128,2048]{1,0:T(8,128)(2,1)S(1)}, bf16[128,2048]{1,0:T(8,128)(2,1)S(1)}, u32[]{:S(2)}, u32[]{:S(2)}) %collective-permute-start.11) | collective-permute-done | bytes 524320 | tf_op jit(solution)/shard_map/ppermute | solution.py:253
  114.4 4.8 %expert_ffn.7 = (bf16[2,64,1024]{2,1,0:T(8,128)(2,1)S(1)}, bf16[2,64,1024]{2,1,0:T(8,128)(2,1)S(1)}, bf16[2,64,1024]{2,1,0:T(8,128)(2,1)S(1)}, bf16[2,64,1024]{2,1,0:T(8,128)(2,1)S(1)}) custom-call(bf16[2,64,2048]{2,1,0:T(8,128)(2,1)S(1)} %bitcast.96, bf16[2,64,2048]{2,1,0:T(8,128)(2,1)S(1)} %bitcast.65, bf16[2,64,2048]{2,1,0:T(8,128)(2,1)S(1)} %bitcast.66, ...), custom_call_target="tpu_custom_call" | custom-call | flops 6000000000 | bytes 12582912 | tf_op jit(solution)/shard_map/expert_ffn/pallas_call | solution.py:195
  119.2 5.0 %collective-permute-done = bf16[128,2048]{1,0:T(8,128)(2,1)S(1)} collective-permute-done((bf16[128,2048]{1,0:T(8,128)(2,1)S(1)}, bf16[128,2048]{1,0:T(8,128)(2,1)S(1)}, u32[]{:S(2)}, u32[]{:S(2)}) %collective-permute-start) | collective-permute-done | bytes 524320 | tf_op jit(solution)/shard_map/ppermute | solution.py:253
  128.6 4.6 %expert_ffn.5 = (bf16[2,64,2048]{2,1,0:T(8,128)(2,1)S(1)}, bf16[2,64,2048]{2,1,0:T(8,128)(2,1)S(1)}) custom-call(bf16[2,64,2048]{2,1,0:T(8,128)(2,1)S(1)} %bitcast.95, bf16[2,64,2048]{2,1,0:T(8,128)(2,1)S(1)} %bitcast.64, f32[1,2048]{1,0:T(1,128)S(1)} %bitcast.88, bf16[2,2048,256]{2,1,0:T(8,128)(2,1)S(1)} %copy-done, bf16[2,2048,256]{2,1,0:T(8,128)(2,1)S(1)} %copy-done.1, ...), custom_call_target="tpu_custom_call" | custom-call | flops 6000000000 | bytes 12582912 | tf_op jit(solution)/shard_map/expert_ffn/pallas_call | solution.py:195
  134.0 12.5 %collective-permute-done.37 = bf16[128,1024]{1,0:T(8,128)(2,1)S(1)} collective-permute-done((bf16[128,1024]{1,0:T(8,128)(2,1)S(1)}, bf16[128,1024]{1,0:T(8,128)(2,1)S(1)}, u32[]{:S(2)}, u32[]{:S(2)}) %collective-permute-start.37) | collective-permute-done | bytes 262176 | tf_op jit(solution)/shard_map/ppermute | solution.py:253
  146.5 3.1 %collective-permute-start.15 = (bf16[128,1024]{1,0:T(8,128)(2,1)S(1)}, bf16[128,1024]{1,0:T(8,128)(2,1)S(1)}, u32[]{:S(2)}, u32[]{:S(2)}) collective-permute-start(bf16[128,1024]{1,0:T(8,128)(2,1)S(1)} %bitcast.82), channel_id=1, source_target_pairs={{0,2},{2,0},{12,14},{14,12},{1,3},{3,1},{13,15},{15,13},{16,18},{1... | collective-permute-start | bytes 786440 | tf_op jit(solution)/shard_map/ppermute | solution.py:253
  153.1 4.9 %expert_ffn.9 = (bf16[2,64,1024]{2,1,0:T(8,128)(2,1)S(1)}, bf16[2,64,1024]{2,1,0:T(8,128)(2,1)S(1)}, bf16[2,64,1024]{2,1,0:T(8,128)(2,1)S(1)}, bf16[2,64,1024]{2,1,0:T(8,128)(2,1)S(1)}) custom-call(bf16[2,64,2048]{2,1,0:T(8,128)(2,1)S(1)} %bitcast.94, bf16[2,64,2048]{2,1,0:T(8,128)(2,1)S(1)} %bitcast.60, bf16[2,64,2048]{2,1,0:T(8,128)(2,1)S(1)} %bitcast.61, ...), custom_call_target="tpu_custom_call" | custom-call | flops 6000000000 | bytes 12582912 | tf_op jit(solution)/shard_map/expert_ffn/pallas_call | solution.py:195
  160.0 3.4 %collective-permute-start.38 = (bf16[128,1024]{1,0:T(8,128)(2,1)S(1)}, bf16[128,1024]{1,0:T(8,128)(2,1)S(1)}, u32[]{:S(2)}, u32[]{:S(2)}) collective-permute-start(bf16[128,1024]{1,0:T(8,128)(2,1)S(1)} %collective-permute-done.37), channel_id=1, source_target_pairs={{0,4},{2,6},{12,8},{14,10},{1,5},{3,7},{13,9},{15,11},{16,20},{18,... | collective-permute-start | bytes 786440 | tf_op jit(solution)/shard_map/ppermute | solution.py:253
  164.8 3.1 %collective-permute-start.42 = (bf16[128,1024]{1,0:T(8,128)(2,1)S(1)}, bf16[128,1024]{1,0:T(8,128)(2,1)S(1)}, u32[]{:S(2)}, u32[]{:S(2)}) collective-permute-start(bf16[128,1024]{1,0:T(8,128)(2,1)S(1)} %bitcast.80), channel_id=1, source_target_pairs={{0,2},{2,0},{12,14},{14,12},{1,3},{3,1},{13,15},{15,13},{16,18},{1... | collective-permute-start | bytes 786440 | tf_op jit(solution)/shard_map/ppermute | solution.py:253
  170.8 3.3 %collective-permute-done.16.refs_3_ = bf16[128,1024]{1,0:T(8,128)(2,1)S(1)} collective-permute-done((bf16[128,1024]{1,0:T(8,128)(2,1)S(1)}, bf16[128,1024]{1,0:T(8,128)(2,1)S(1)}, u32[]{:S(2)}, u32[]{:S(2)}) %collective-permute-start.16) | collective-permute-done | bytes 262176 | tf_op jit(solution)/shard_map/ppermute | solution.py:253
  174.1 2.8 %collective-permute-start.29 = (bf16[128,1024]{1,0:T(8,128)(2,1)S(1)}, bf16[128,1024]{1,0:T(8,128)(2,1)S(1)}, u32[]{:S(2)}, u32[]{:S(2)}) collective-permute-start(bf16[128,1024]{1,0:T(8,128)(2,1)S(1)} %bitcast.71), channel_id=1, source_target_pairs={{0,2},{2,0},{12,14},{14,12},{1,3},{3,1},{13,15},{15,13},{16,18},{1... | collective-permute-start | bytes 786440 | tf_op jit(solution)/shard_map/ppermute | solution.py:253
  180.6 9.0 %collective-permute-done.42 = bf16[128,1024]{1,0:T(8,128)(2,1)S(1)} collective-permute-done((bf16[128,1024]{1,0:T(8,128)(2,1)S(1)}, bf16[128,1024]{1,0:T(8,128)(2,1)S(1)}, u32[]{:S(2)}, u32[]{:S(2)}) %collective-permute-start.42) | collective-permute-done | bytes 262176 | tf_op jit(solution)/shard_map/ppermute | solution.py:253
  199.9 3.2 %collective-permute-done.28.refs_2_ = bf16[128,1024]{1,0:T(8,128)(2,1)S(1)} collective-permute-done((bf16[128,1024]{1,0:T(8,128)(2,1)S(1)}, bf16[128,1024]{1,0:T(8,128)(2,1)S(1)}, u32[]{:S(2)}, u32[]{:S(2)}) %collective-permute-start.28) | collective-permute-done | bytes 262176 | tf_op jit(solution)/shard_map/ppermute | solution.py:253
  208.3 20.2 %collective-permute-start.47 = (bf16[256,512]{1,0:T(8,128)(2,1)S(1)}, bf16[256,512]{1,0:T(8,128)(2,1)S(1)}, u32[]{:S(2)}, u32[]{:S(2)}) collective-permute-start(bf16[256,512]{1,0:T(8,128)(2,1)S(1)} %add_convert_fusion), channel_id=1, source_target_pairs={{0,4},{2,6},{4,0},{6,2},{8,12},{10,14},{12,8},{14,10},{1,5},{3,7},... | collective-permute-start | bytes 786440 | tf_op jit(solution)/shard_map/ppermute | solution.py:253
  228.6 4.6 %collective-permute-start.45 = (bf16[256,512]{1,0:T(8,128)(2,1)S(1)}, bf16[256,512]{1,0:T(8,128)(2,1)S(1)}, u32[]{:S(2)}, u32[]{:S(2)}) collective-permute-start(bf16[256,512]{1,0:T(8,128)(2,1)S(1)} %add_convert_fusion.1), channel_id=1, source_target_pairs={{0,4},{2,6},{4,0},{6,2},{8,12},{10,14},{12,8},{14,10},{1,5},{3,7},... | collective-permute-start | bytes 786440 | tf_op jit(solution)/shard_map/ppermute | solution.py:253
  237.0 3.4 %collective-permute-done.45.refs_2_ = bf16[256,512]{1,0:T(8,128)(2,1)S(1)} collective-permute-done((bf16[256,512]{1,0:T(8,128)(2,1)S(1)}, bf16[256,512]{1,0:T(8,128)(2,1)S(1)}, u32[]{:S(2)}, u32[]{:S(2)}) %collective-permute-start.45) | collective-permute-done | bytes 262176 | tf_op jit(solution)/shard_map/ppermute | solution.py:253
  241.1 3.4 %collective-permute-done.34.refs_2_ = bf16[256,512]{1,0:T(8,128)(2,1)S(1)} collective-permute-done((bf16[256,512]{1,0:T(8,128)(2,1)S(1)}, bf16[256,512]{1,0:T(8,128)(2,1)S(1)}, u32[]{:S(2)}, u32[]{:S(2)}) %collective-permute-start.34) | collective-permute-done | bytes 262176 | tf_op jit(solution)/shard_map/ppermute | solution.py:253
  (123 shorter events, 66.5 us)
Async XLA Ops:
  0.0 33.2 %collective-permute-start.19 = (bf16[256,2048]{1,0:T(8,128)(2,1)}, bf16[256,2048]{1,0:T(8,128)(2,1)S(1)}, u32[]{:S(2)}, u32[]{:S(2)}) collective-permute-start(bf16[256,2048]{1,0:T(8,128)(2,1)} %x_ref.1), channel_id=1, source_target_pairs={{0,4},{2,6},{4,0},{6,2},{8,12},{10,14},{12,8},{14,10},{1,5},{3,7},... | collective-permute-start | bytes 3145736 | tf_op jit(solution)/shard_map/ppermute | solution.py:253
  3.1 47.1 %collective-permute-start.1 = (bf16[2,2048,256]{2,1,0:T(8,128)(2,1)}, bf16[2,2048,256]{2,1,0:T(8,128)(2,1)S(1)}, u32[]{:S(2)}, u32[]{:S(2)}) collective-permute-start(bf16[2,2048,256]{2,1,0:T(8,128)(2,1)} %refs_5_.7), channel_id=1, source_target_pairs={{0,1},{1,0},{2,3},{3,2},{4,5},{5,4},{6,7},{7,6},{8,9},{9,8},{10,11... | collective-permute-start | bytes 6291464 | tf_op jit(solution)/shard_map/ppermute | solution.py:259
  3.1 48.4 %collective-permute-start.2 = (bf16[2,2048,256]{2,1,0:T(8,128)(2,1)}, bf16[2,2048,256]{2,1,0:T(8,128)(2,1)}, u32[]{:S(2)}, u32[]{:S(2)}) collective-permute-start(bf16[2,2048,256]{2,1,0:T(8,128)(2,1)} %refs_6_.3), channel_id=1, source_target_pairs={{0,1},{1,0},{2,3},{3,2},{4,5},{5,4},{6,7},{7,6},{8,9},{9,8},{10,11... | collective-permute-start | bytes 6291464 | tf_op jit(solution)/shard_map/ppermute | solution.py:259
  3.6 49.2 %collective-permute-start.3 = (bf16[2,256,2048]{2,1,0:T(8,128)(2,1)}, bf16[2,256,2048]{2,1,0:T(8,128)(2,1)}, u32[]{:S(2)}, u32[]{:S(2)}) collective-permute-start(bf16[2,256,2048]{2,1,0:T(8,128)(2,1)} %refs_7_.3), channel_id=1, source_target_pairs={{0,1},{1,0},{2,3},{3,2},{4,5},{5,4},{6,7},{7,6},{8,9},{9,8},{10,11... | collective-permute-start | bytes 6291464 | tf_op jit(solution)/shard_map/ppermute | solution.py:259
  4.9 20.9 %collective-permute-start.22 = (f32[4,256]{1,0:T(4,128)S(1)}, f32[4,256]{1,0:T(4,128)S(1)}, u32[]{:S(2)}, u32[]{:S(2)}) collective-permute-start(f32[4,256]{1,0:T(4,128)S(1)} %pad_maximum_fusion.m_ref), channel_id=1, source_target_pairs={{12,4},{14,6},{0,8},{2,10},{13,5},{15,7},{1,9},{3,11},{28,20},{30,... | collective-permute-start | bytes 12296 | tf_op jit(solution)/shard_map/ppermute | solution.py:253
  43.3 82.2 %collective-permute-start.5 = (bf16[2048,256]{1,0:T(8,128)(2,1)S(1)}, bf16[2048,256]{1,0:T(8,128)(2,1)S(1)}, u32[]{:S(2)}, u32[]{:S(2)}) collective-permute-start(bf16[2048,256]{1,0:T(8,128)(2,1)S(1)} %copy-done.5), channel_id=1, source_target_pairs={{0,1},{1,0},{2,3},{3,2},{4,5},{5,4},{6,7},{7,6},{8,9},{9,8},{10,11... | collective-permute-start | bytes 3145736 | tf_op jit(solution)/shard_map/ppermute | solution.py:259
  50.1 76.1 %collective-permute-start.6 = (bf16[2048,256]{1,0:T(8,128)(2,1)S(1)}, bf16[2048,256]{1,0:T(8,128)(2,1)S(1)}, u32[]{:S(2)}, u32[]{:S(2)}) collective-permute-start(bf16[2048,256]{1,0:T(8,128)(2,1)S(1)} %copy-done.6), channel_id=1, source_target_pairs={{0,1},{1,0},{2,3},{3,2},{4,5},{5,4},{6,7},{7,6},{8,9},{9,8},{10,11... | collective-permute-start | bytes 3145736 | tf_op jit(solution)/shard_map/ppermute | solution.py:259
  50.2 51.3 %collective-permute-start.10 = (bf16[128,2048]{1,0:T(8,128)(2,1)S(1)}, bf16[128,2048]{1,0:T(8,128)(2,1)S(1)}, u32[]{:S(2)}, u32[]{:S(2)}) collective-permute-start(bf16[128,2048]{1,0:T(8,128)(2,1)S(1)} %get-tuple-element.38), channel_id=1, source_target_pairs={{4,0},{6,2},{8,12},{10,14},{5,1},{7,3},{9,13},{11,15},{20,16},{22,... | collective-permute-start | bytes 1572872 | tf_op jit(solution)/shard_map/ppermute | solution.py:253
  51.5 61.6 %collective-permute-start.11 = (bf16[128,2048]{1,0:T(8,128)(2,1)S(1)}, bf16[128,2048]{1,0:T(8,128)(2,1)S(1)}, u32[]{:S(2)}, u32[]{:S(2)}) collective-permute-start(bf16[128,2048]{1,0:T(8,128)(2,1)S(1)} %get-tuple-element.39), channel_id=1, source_target_pairs={{4,2},{6,0},{8,14},{10,12},{5,3},{7,1},{9,15},{11,13},{20,18},{22,... | collective-permute-start | bytes 1572872 | tf_op jit(solution)/shard_map/ppermute | solution.py:253
  52.8 60.3 %collective-permute-start.12 = (bf16[128,2048]{1,0:T(8,128)(2,1)S(1)}, bf16[128,2048]{1,0:T(8,128)(2,1)S(1)}, u32[]{:S(2)}, u32[]{:S(2)}) collective-permute-start(bf16[128,2048]{1,0:T(8,128)(2,1)S(1)} %get-tuple-element.40), channel_id=1, source_target_pairs={{4,6},{6,4},{8,10},{10,8},{5,7},{7,5},{9,11},{11,9},{20,22},{22,20... | collective-permute-start | bytes 1572872 | tf_op jit(solution)/shard_map/ppermute | solution.py:253
  101.4 22.8 %collective-permute-start = (bf16[128,2048]{1,0:T(8,128)(2,1)S(1)}, bf16[128,2048]{1,0:T(8,128)(2,1)S(1)}, u32[]{:S(2)}, u32[]{:S(2)}) collective-permute-start(bf16[128,2048]{1,0:T(8,128)(2,1)S(1)} %get-tuple-element.34), channel_id=1, source_target_pairs={{0,2},{2,0},{4,6},{6,4},{8,10},{10,8},{12,14},{14,12},{1,3},{3,1},... | collective-permute-start | bytes 1572872 | tf_op jit(solution)/shard_map/ppermute | solution.py:253
  113.1 36.4 %collective-permute-start.24 = (bf16[128,2048]{1,0:T(8,128)(2,1)S(1)}, bf16[128,2048]{1,0:T(8,128)(2,1)S(1)}, u32[]{:S(2)}, u32[]{:S(2)}) collective-permute-start(bf16[128,2048]{1,0:T(8,128)(2,1)S(1)} %get-tuple-element.49), channel_id=1, source_target_pairs={{4,0},{6,2},{8,12},{10,14},{5,1},{7,3},{9,13},{11,15},{20,16},{22,... | collective-permute-start | bytes 1572872 | tf_op jit(solution)/shard_map/ppermute | solution.py:253
  124.2 26.0 %collective-permute-start.25 = (bf16[128,2048]{1,0:T(8,128)(2,1)S(1)}, bf16[128,2048]{1,0:T(8,128)(2,1)S(1)}, u32[]{:S(2)}, u32[]{:S(2)}) collective-permute-start(bf16[128,2048]{1,0:T(8,128)(2,1)S(1)} %get-tuple-element.50), channel_id=1, source_target_pairs={{4,2},{6,0},{8,14},{10,12},{5,3},{7,1},{9,15},{11,13},{20,18},{22,... | collective-permute-start | bytes 1572872 | tf_op jit(solution)/shard_map/ppermute | solution.py:253
  125.5 26.0 %collective-permute-start.26 = (bf16[128,2048]{1,0:T(8,128)(2,1)S(1)}, bf16[128,2048]{1,0:T(8,128)(2,1)S(1)}, u32[]{:S(2)}, u32[]{:S(2)}) collective-permute-start(bf16[128,2048]{1,0:T(8,128)(2,1)S(1)} %get-tuple-element.51), channel_id=1, source_target_pairs={{4,6},{6,4},{8,10},{10,8},{5,7},{7,5},{9,11},{11,9},{20,22},{22,20... | collective-permute-start | bytes 1572872 | tf_op jit(solution)/shard_map/ppermute | solution.py:253
  133.3 24.7 %collective-permute-start.35 = (bf16[128,1024]{1,0:T(8,128)(2,1)S(1)}, bf16[128,1024]{1,0:T(8,128)(2,1)S(1)}, u32[]{:S(2)}, u32[]{:S(2)}) collective-permute-start(bf16[128,1024]{1,0:T(8,128)(2,1)S(1)} %bitcast.85), channel_id=1, source_target_pairs={{4,6},{6,4},{8,10},{10,8},{5,7},{7,5},{9,11},{11,9},{20,22},{22,20... | collective-permute-start | bytes 786440 | tf_op jit(solution)/shard_map/ppermute | solution.py:253
  157.9 20.4 %collective-permute-start.21 = (bf16[128,2048]{1,0:T(8,128)(2,1)S(1)}, bf16[128,2048]{1,0:T(8,128)(2,1)S(1)}, u32[]{:S(2)}, u32[]{:S(2)}) collective-permute-start(bf16[128,2048]{1,0:T(8,128)(2,1)S(1)} %bitcast.58), channel_id=1, source_target_pairs={{0,2},{2,0},{4,6},{6,4},{8,10},{10,8},{12,14},{14,12},{1,3},{3,1},... | collective-permute-start | bytes 1572872 | tf_op jit(solution)/shard_map/ppermute | solution.py:253
  158.9 33.1 %collective-permute-start.4 = (bf16[128,2048]{1,0:T(8,128)(2,1)S(1)}, bf16[128,2048]{1,0:T(8,128)(2,1)S(1)}, u32[]{:S(2)}, u32[]{:S(2)}) collective-permute-start(bf16[128,2048]{1,0:T(8,128)(2,1)S(1)} %bitcast.59), channel_id=1, source_target_pairs={{0,2},{2,0},{4,6},{6,4},{8,10},{10,8},{12,14},{14,12},{1,3},{3,1},... | collective-permute-start | bytes 1572872 | tf_op jit(solution)/shard_map/ppermute | solution.py:253
  164.8 24.9 %collective-permute-start.42 = (bf16[128,1024]{1,0:T(8,128)(2,1)S(1)}, bf16[128,1024]{1,0:T(8,128)(2,1)S(1)}, u32[]{:S(2)}, u32[]{:S(2)}) collective-permute-start(bf16[128,1024]{1,0:T(8,128)(2,1)S(1)} %bitcast.80), channel_id=1, source_target_pairs={{0,2},{2,0},{12,14},{14,12},{1,3},{3,1},{13,15},{15,13},{16,18},{1... | collective-permute-start | bytes 786440 | tf_op jit(solution)/shard_map/ppermute | solution.py:253
  170.1 22.5 %collective-permute-start.40 = (bf16[128,1024]{1,0:T(8,128)(2,1)S(1)}, bf16[128,1024]{1,0:T(8,128)(2,1)S(1)}, u32[]{:S(2)}, u32[]{:S(2)}) collective-permute-start(bf16[128,1024]{1,0:T(8,128)(2,1)S(1)} %bitcast.81), channel_id=1, source_target_pairs={{4,6},{6,4},{8,10},{10,8},{5,7},{7,5},{9,11},{11,9},{20,22},{22,20... | collective-permute-start | bytes 786440 | tf_op jit(solution)/shard_map/ppermute | solution.py:253
  196.3 39.8 %collective-permute-start.39 = (bf16[256,1024]{1,0:T(8,128)(2,1)S(1)}, bf16[256,1024]{1,0:T(8,128)(2,1)S(1)}, u32[]{:S(2)}, u32[]{:S(2)}) collective-permute-start(bf16[256,1024]{1,0:T(8,128)(2,1)S(1)} %combine_piece.9), channel_id=1, source_target_pairs={{4,8},{6,10},{8,4},{10,6},{5,9},{7,11},{9,5},{11,7},{20,24},{22,26... | collective-permute-start | bytes 1572872 | tf_op jit(solution)/shard_map/ppermute | solution.py:253
  199.2 41.9 %collective-permute-start.17 = (bf16[256,1024]{1,0:T(8,128)(2,1)S(1)}, bf16[256,1024]{1,0:T(8,128)(2,1)S(1)}, u32[]{:S(2)}, u32[]{:S(2)}) collective-permute-start(bf16[256,1024]{1,0:T(8,128)(2,1)S(1)} %combine_piece.6), channel_id=1, source_target_pairs={{4,8},{6,10},{8,4},{10,6},{5,9},{7,11},{9,5},{11,7},{20,24},{22,26... | collective-permute-start | bytes 1572872 | tf_op jit(solution)/shard_map/ppermute | solution.py:253
  206.4 22.2 %collective-permute-start.33 = (bf16[256,512]{1,0:T(8,128)(2,1)S(1)}, bf16[256,512]{1,0:T(8,128)(2,1)S(1)}, u32[]{:S(2)}, u32[]{:S(2)}) collective-permute-start(bf16[256,512]{1,0:T(8,128)(2,1)S(1)} %combine_piece.8), channel_id=1, source_target_pairs={{4,8},{6,10},{8,4},{10,6},{5,9},{7,11},{9,5},{11,7},{20,24},{22,26... | collective-permute-start | bytes 786440 | tf_op jit(solution)/shard_map/ppermute | solution.py:253
  207.5 25.7 %collective-permute-start.31 = (bf16[256,512]{1,0:T(8,128)(2,1)S(1)}, bf16[256,512]{1,0:T(8,128)(2,1)S(1)}, u32[]{:S(2)}, u32[]{:S(2)}) collective-permute-start(bf16[256,512]{1,0:T(8,128)(2,1)S(1)} %combine_piece.7), channel_id=1, source_target_pairs={{4,8},{6,10},{8,4},{10,6},{5,9},{7,11},{9,5},{11,7},{20,24},{22,26... | collective-permute-start | bytes 786440 | tf_op jit(solution)/shard_map/ppermute | solution.py:253
  208.3 27.9 %collective-permute-start.47 = (bf16[256,512]{1,0:T(8,128)(2,1)S(1)}, bf16[256,512]{1,0:T(8,128)(2,1)S(1)}, u32[]{:S(2)}, u32[]{:S(2)}) collective-permute-start(bf16[256,512]{1,0:T(8,128)(2,1)S(1)} %add_convert_fusion), channel_id=1, source_target_pairs={{0,4},{2,6},{4,0},{6,2},{8,12},{10,14},{12,8},{14,10},{1,5},{3,7},... | collective-permute-start | bytes 786440 | tf_op jit(solution)/shard_map/ppermute | solution.py:253
  (33 other events, 395.2 us)

commit v3 on v2

--- a/solution.py
+++ b/solution.py
@@ -9,6 +9,7 @@
 
 
 CHUNKS = 4
+SIDE = 1
 SMALL = pltpu.CompilerParams(vmem_limit_bytes=8 * 1024 * 1024)
 LARGE = pltpu.CompilerParams(vmem_limit_bytes=16 * 1024 * 1024)
 BF, F32 = jnp.bfloat16, jnp.float32
@@ -121,9 +122,13 @@
     )(meta, experts)
 
 
-def column_piece(arrays, rows, wide, piece, pieces):
-    inside = piece % (pieces // len(arrays))
-    return arrays[piece * len(arrays) // pieces], pl.BlockSpec((rows, wide), lambda i: (0, inside))
+def column_piece(arrays, rows, wide, piece):
+    low = piece * wide
+    for a in arrays:
+        if low < a.shape[1]:
+            inside = low // wide
+            return a, pl.BlockSpec((rows, wide), lambda i: (0, inside))
+        low -= a.shape[1]
 
 
 def combine_piece(matrix, parts, piece, pieces):
@@ -138,7 +143,7 @@
         total = total + jnp.dot(m_ref[:, count:], stacked, preferred_element_type=F32)
         refs[-1][...] = total.astype(BF)
 
-    args, specs = zip(*[column_piece(p, rows, wide, piece, pieces) for p in parts])
+    args, specs = zip(*[column_piece(p, rows, wide, piece) for p in parts])
     return pl.pallas_call(
         kernel,
         grid=(1,),
@@ -156,7 +161,7 @@
     n = len(parts)
     flat = [a for p in parts for a in p]
     count = len(flat)
-    wides = [d // c for counts in splits for c in counts for _ in range(c)]
+    wides = [w for ways in splits for way in ways for w in way]
     total = len(wides)
 
     def kernel(*refs):
@@ -184,11 +189,11 @@
             y = y + jnp.dot(hidden[1], w_in[5][e], preferred_element_type=F32)
             at = 0
             for i in range(n):
-                for pieces in splits[i]:
-                    wide = d // pieces
-                    for c in range(pieces):
-                        piece = y[i * rows : (i + 1) * rows, c * wide : (c + 1) * wide]
-                        outs[at][e] = piece.astype(dtype)
+                for way in splits[i]:
+                    low = 0
+                    for wide in way:
+                        outs[at][e] = y[i * rows : (i + 1) * rows, low : low + wide].astype(dtype)
+                        low += wide
                         at += 1
 
     whole = pl.BlockSpec(memory_space=pltpu.VMEM)
@@ -208,7 +213,7 @@
     n, d = base.shape
     wide = d // chunks
 
-    args, specs = zip(*[column_piece(arrays, n, wide, chunk, chunks) for arrays in [[base]] + lists])
+    args, specs = zip(*[column_piece(arrays, n, wide, chunk) for arrays in [[base]] + lists])
     args, specs = list(args), list(specs)
     count = len(args)
     alias = {}
@@ -328,14 +333,14 @@
         outs = expert_ffn([[shaped(a) for a in part] for part in sources], gain, routed_w, splits, BF)
         outs = [a.reshape(local_exp * cap, a.shape[-1]) for a in outs]
         result, at = [], 0
-        for counts in splits:
+        for ways in splits:
             result.append([])
-            for c in counts:
-                result[-1].append(outs[at : at + c])
-                at += c
+            for way in ways:
+                result[-1].append(outs[at : at + len(way)])
+                at += len(way)
         return result
 
-    shared = expert_ffn([[tokens[None]]], gain, s_own + s_others, [(1,)], F32)[0][0]
+    shared = expert_ffn([[tokens[None]]], gain, s_own + s_others, [[(width,)]], F32)[0][0]
 
     def plus(a, b):
         return (a.astype(F32) + b.astype(F32)).astype(BF)
@@ -344,13 +349,18 @@
     for s, block in enumerate(slots):
         rows = compact(block, metas[s], here, topk, local_exp, cap)
         got = [across(rows[k], k) for k in range(1, inner)]
-        outs = experts([[rows[0]]] + [[a] for a in got], [(1,)] * inner)
-        outs = [o[0][0] for o in outs]
-        parts = [outs[0]] + [across(outs[k], k) for k in range(1, inner)]
-        if s == 0:
-            sums.append(combine(metas[s], here, topk, parts, cap, [shared], F32, 1))
-        else:
-            sums.append(combine(metas[s], here, topk, parts, cap, [], BF, chunks))
+        count = 1 if s == 0 else SIDE
+        outs = experts([[rows[0]]] + [[a] for a in got], [[(width // count,) * count]] * inner)
+        outs = [o[0] for o in outs]
+        back = [[across(a, k) for a in outs[k]] for k in range(1, inner)]
+        made = []
+        for c in range(count):
+            parts = [outs[0][c]] + [b[c] for b in back]
+            if s == 0:
+                made += combine(metas[s], here, topk, parts, cap, [shared], F32, 1)
+            else:
+                made += combine(metas[s], here, topk, parts, cap, [], BF, chunks // count)
+        sums.append(made)
 
     arrived = [[] for _ in slots]
     for j, block in enumerate(tops):
@@ -362,8 +372,8 @@
                 if d or k:
                     mine[k].append(send(rows[d * inner + k], outward[d, k]))
         pieces = max(1, chunks // 2) if j == 0 else chunks
-        halves = min(pieces, 2)
-        results = experts(mine, [(halves,)] * inner)
+        even = (width // min(pieces, 2),) * min(pieces, 2)
+        results = experts(mine, [[even]] + [[(width,), even]] * (inner - 1))
 
         def row(arrays, d, k):
             ends = [edge[i] + away[i] * d for i in (half - 1, half)]
@@ -373,7 +383,7 @@
         near = [results[0][0]] + [row(results[k][0], 0, k) for k in range(1, inner)]
         far = []
         for d in range(1, half):
-            crossed = [results[0][0]] + [row(results[k][0], d, k) for k in range(1, inner)]
+            crossed = [results[0][0]] + [row(results[k][1], d, k) for k in range(1, inner)]
             for part in crossed:
                 far.append([send(a, inward[d, 0]) for a in part])
         got = []

time: 249 us -> 253 us (1.016)
  waiting for transfers between devices: 120 us -> 124 us
    ppermute x42 -> x40, waiting for transfers between devices: 120 us -> 124 us  [send(): return lax.ppermute(x, 'ep', pairs)]
    ppermute x42 -> x40, starting transfers between devices: 86.1 us -> 86.3 us  [send(): return lax.ppermute(x, 'ep', pairs)]
  transfers between devices with their start and end apart: 48 -> 46, of which waited for: 16 -> 19; matrix products, arithmetic and copies ran while one was open for 1% -> 1% of each run, Pallas kernels for 15% -> 14%
where the time goes in v3:
time: 253 us; the launch traced here: 252 us
  waiting for transfers between devices  124 us (49%)
  starting transfers between devices  86.9 us (34%)
  Pallas kernels  37 us (15%)
    ppermute x40, waiting for transfers between devices, send(): return lax.ppermute(x, 'ep', pairs)  124 us
    ppermute x40, starting transfers between devices, send(): return lax.ppermute(x, 'ep', pairs)  86.3 us
    pallas_call x5, Pallas kernels, expert_ffn(): pl.pallas_call(kernel, in_specs=[whole] * (count + 7), out_specs=[whole]...  21.1 us
    pallas_call x4, Pallas kernels, compact(): pl.pallas_call(kernel, grid=(steps,), in_specs=[pl.BlockSpec((n, wide), l...  6.86 us
  transfers between devices with their start and end apart: 46, of which 19 were waited for; matrix products, arithmetic and copies ran while one was open for 1% of the time, Pallas kernels for 14%

profile of v3, /device:TPU:0, one launch (start us, length us, event | category | flops | bytes accessed | tf_op | source)
XLA Modules:
  0.0 251.7 jit_solution(11047875252525497896)
XLA Ops:
  0.0 3.1 %collective-permute-start.19 = (bf16[256,2048]{1,0:T(8,128)(2,1)}, bf16[256,2048]{1,0:T(8,128)(2,1)S(1)}, u32[]{:S(2)}, u32[]{:S(2)}) collective-permute-start(bf16[256,2048]{1,0:T(8,128)(2,1)} %x_ref.1), channel_id=1, source_target_pairs={{0,4},{2,6},{4,0},{6,2},{8,12},{10,14},{12,8},{14,10},{1,5},{3,7},... | collective-permute-start | bytes 3145736 | tf_op jit(solution)/shard_map/ppermute | solution.py:258
  4.9 4.5 %collective-permute-start.22 = (f32[4,256]{1,0:T(4,128)S(1)}, f32[4,256]{1,0:T(4,128)S(1)}, u32[]{:S(2)}, u32[]{:S(2)}) collective-permute-start(f32[4,256]{1,0:T(4,128)S(1)} %pad_maximum_fusion.m_ref), channel_id=1, source_target_pairs={{12,4},{14,6},{0,8},{2,10},{13,5},{15,7},{1,9},{3,11},{28,20},{30,... | collective-permute-start | bytes 12296 | tf_op jit(solution)/shard_map/ppermute | solution.py:258
  9.4 16.4 %collective-permute-done.22.m_ref = f32[4,256]{1,0:T(4,128)S(1)} collective-permute-done((f32[4,256]{1,0:T(4,128)S(1)}, f32[4,256]{1,0:T(4,128)S(1)}, u32[]{:S(2)}, u32[]{:S(2)}) %collective-permute-start.22) | collective-permute-done | bytes 4128 | tf_op jit(solution)/shard_map/ppermute | solution.py:258
  25.8 3.4 %collective-permute-start.18 = (f32[4,256]{1,0:T(4,128)S(1)}, f32[4,256]{1,0:T(4,128)S(1)}, u32[]{:S(2)}, u32[]{:S(2)}) collective-permute-start(f32[4,256]{1,0:T(4,128)S(1)} %pad_maximum_fusion.m_ref), channel_id=1, source_target_pairs={{0,4},{2,6},{4,0},{6,2},{8,12},{10,14},{12,8},{14,10},{1,5},{3,7},... | collective-permute-start | bytes 12296 | tf_op jit(solution)/shard_map/ppermute | solution.py:258
  45.9 4.2 %collective-permute-done.20 = bf16[128,2048]{1,0:T(8,128)(2,1)S(1)} collective-permute-done((bf16[128,2048]{1,0:T(8,128)(2,1)S(1)}, bf16[128,2048]{1,0:T(8,128)(2,1)S(1)}, u32[]{:S(2)}, u32[]{:S(2)}) %collective-permute-start.20) | collective-permute-done | bytes 524320 | tf_op jit(solution)/shard_map/ppermute | solution.py:258
  53.6 4.7 %expert_ffn.8 = (bf16[2,64,2048]{2,1,0:T(8,128)(2,1)S(1)}, bf16[2,64,2048]{2,1,0:T(8,128)(2,1)S(1)}) custom-call(bf16[2,64,2048]{2,1,0:T(8,128)(2,1)S(1)} %bitcast.97, bf16[2,64,2048]{2,1,0:T(8,128)(2,1)S(1)} %bitcast.66, f32[1,2048]{1,0:T(1,128)S(1)} %bitcast.86, bf16[2,2048,256]{2,1,0:T(8,128)(2,1)S(1)} %copy-done, bf16[2,2048,256]{2,1,0:T(8,128)(2,1)S(1)} %copy-done.1, ...), custom_call_target="tpu_custom_call" | custom-call | flops 6000000000 | bytes 12582912 | tf_op jit(solution)/shard_map/expert_ffn/pallas_call | solution.py:200
  58.2 43.2 %collective-permute-done.10 = bf16[128,2048]{1,0:T(8,128)(2,1)S(1)} collective-permute-done((bf16[128,2048]{1,0:T(8,128)(2,1)S(1)}, bf16[128,2048]{1,0:T(8,128)(2,1)S(1)}, u32[]{:S(2)}, u32[]{:S(2)}) %collective-permute-start.10) | collective-permute-done | bytes 524320 | tf_op jit(solution)/shard_map/ppermute | solution.py:258
  103.0 10.1 %collective-permute-done.11 = bf16[128,2048]{1,0:T(8,128)(2,1)S(1)} collective-permute-done((bf16[128,2048]{1,0:T(8,128)(2,1)S(1)}, bf16[128,2048]{1,0:T(8,128)(2,1)S(1)}, u32[]{:S(2)}, u32[]{:S(2)}) %collective-permute-start.11) | collective-permute-done | bytes 524320 | tf_op jit(solution)/shard_map/ppermute | solution.py:258
  114.4 4.8 %expert_ffn.7 = (bf16[2,64,1024]{2,1,0:T(8,128)(2,1)S(1)}, bf16[2,64,1024]{2,1,0:T(8,128)(2,1)S(1)}, bf16[2,64,2048]{2,1,0:T(8,128)(2,1)S(1)}, bf16[2,64,1024]{2,1,0:T(8,128)(2,1)S(1)}, bf16[2,64,1024]{2,1,0:T(8,128)(2,1)S(1)}) custom-call(bf16[2,64,2048]{2,1,0:T(8,128)(2,1)S(1)} %bitcast.96, bf16[2,64,2048]{2,1,0:T(8,128)(2,1)S(1)} %bitcast.69, ...), custom_call_target="tpu_custom_call" | custom-call | flops 6000000000 | bytes 12582912 | tf_op jit(solution)/shard_map/expert_ffn/pallas_call | solution.py:200
  119.2 5.0 %collective-permute-done = bf16[128,2048]{1,0:T(8,128)(2,1)S(1)} collective-permute-done((bf16[128,2048]{1,0:T(8,128)(2,1)S(1)}, bf16[128,2048]{1,0:T(8,128)(2,1)S(1)}, u32[]{:S(2)}, u32[]{:S(2)}) %collective-permute-start) | collective-permute-done | bytes 524320 | tf_op jit(solution)/shard_map/ppermute | solution.py:258
  128.6 4.6 %expert_ffn.5 = (bf16[2,64,2048]{2,1,0:T(8,128)(2,1)S(1)}, bf16[2,64,2048]{2,1,0:T(8,128)(2,1)S(1)}) custom-call(bf16[2,64,2048]{2,1,0:T(8,128)(2,1)S(1)} %bitcast.95, bf16[2,64,2048]{2,1,0:T(8,128)(2,1)S(1)} %bitcast.68, f32[1,2048]{1,0:T(1,128)S(1)} %bitcast.88, bf16[2,2048,256]{2,1,0:T(8,128)(2,1)S(1)} %copy-done, bf16[2,2048,256]{2,1,0:T(8,128)(2,1)S(1)} %copy-done.1, ...), custom_call_target="tpu_custom_call" | custom-call | flops 6000000000 | bytes 12582912 | tf_op jit(solution)/shard_map/expert_ffn/pallas_call | solution.py:200
  133.3 13.2 %collective-permute-done.36 = bf16[128,1024]{1,0:T(8,128)(2,1)S(1)} collective-permute-done((bf16[128,1024]{1,0:T(8,128)(2,1)S(1)}, bf16[128,1024]{1,0:T(8,128)(2,1)S(1)}, u32[]{:S(2)}, u32[]{:S(2)}) %collective-permute-start.36) | collective-permute-done | bytes 262176 | tf_op jit(solution)/shard_map/ppermute | solution.py:258
  147.8 3.1 %collective-permute-start.15 = (bf16[128,1024]{1,0:T(8,128)(2,1)S(1)}, bf16[128,1024]{1,0:T(8,128)(2,1)S(1)}, u32[]{:S(2)}, u32[]{:S(2)}) collective-permute-start(bf16[128,1024]{1,0:T(8,128)(2,1)S(1)} %bitcast.83), channel_id=1, source_target_pairs={{0,2},{2,0},{12,14},{14,12},{1,3},{3,1},{13,15},{15,13},{16,18},{1... | collective-permute-start | bytes 786440 | tf_op jit(solution)/shard_map/ppermute | solution.py:258
  153.7 4.9 %expert_ffn.9 = (bf16[2,64,1024]{2,1,0:T(8,128)(2,1)S(1)}, bf16[2,64,1024]{2,1,0:T(8,128)(2,1)S(1)}, bf16[2,64,2048]{2,1,0:T(8,128)(2,1)S(1)}, bf16[2,64,1024]{2,1,0:T(8,128)(2,1)S(1)}, bf16[2,64,1024]{2,1,0:T(8,128)(2,1)S(1)}) custom-call(bf16[2,64,2048]{2,1,0:T(8,128)(2,1)S(1)} %bitcast.93, bf16[2,64,2048]{2,1,0:T(8,128)(2,1)S(1)} %bitcast.64, ...), custom_call_target="tpu_custom_call" | custom-call | flops 6000000000 | bytes 12582912 | tf_op jit(solution)/shard_map/expert_ffn/pallas_call | solution.py:200
  161.4 2.8 %collective-permute-start.40 = (bf16[128,1024]{1,0:T(8,128)(2,1)S(1)}, bf16[128,1024]{1,0:T(8,128)(2,1)S(1)}, u32[]{:S(2)}, u32[]{:S(2)}) collective-permute-start(bf16[128,1024]{1,0:T(8,128)(2,1)S(1)} %bitcast.84), channel_id=1, source_target_pairs={{0,2},{2,0},{12,14},{14,12},{1,3},{3,1},{13,15},{15,13},{16,18},{1... | collective-permute-start | bytes 786440 | tf_op jit(solution)/shard_map/ppermute | solution.py:258
  167.9 5.5 %collective-permute-done.21.refs_1_ = bf16[128,2048]{1,0:T(8,128)(2,1)S(1)} collective-permute-done((bf16[128,2048]{1,0:T(8,128)(2,1)S(1)}, bf16[128,2048]{1,0:T(8,128)(2,1)S(1)}, u32[]{:S(2)}, u32[]{:S(2)}) %collective-permute-start.21) | collective-permute-done | bytes 524320 | tf_op jit(solution)/shard_map/ppermute | solution.py:258
  174.7 2.8 %collective-permute-start.29 = (bf16[128,1024]{1,0:T(8,128)(2,1)S(1)}, bf16[128,1024]{1,0:T(8,128)(2,1)S(1)}, u32[]{:S(2)}, u32[]{:S(2)}) collective-permute-start(bf16[128,1024]{1,0:T(8,128)(2,1)S(1)} %bitcast.82), channel_id=1, source_target_pairs={{0,2},{2,0},{12,14},{14,12},{1,3},{3,1},{13,15},{15,13},{16,18},{1... | collective-permute-start | bytes 786440 | tf_op jit(solution)/shard_map/ppermute | solution.py:258
  178.5 6.2 %collective-permute-done.4.refs_1_ = bf16[128,2048]{1,0:T(8,128)(2,1)S(1)} collective-permute-done((bf16[128,2048]{1,0:T(8,128)(2,1)S(1)}, bf16[128,2048]{1,0:T(8,128)(2,1)S(1)}, u32[]{:S(2)}, u32[]{:S(2)}) %collective-permute-start.4) | collective-permute-done | bytes 524320 | tf_op jit(solution)/shard_map/ppermute | solution.py:258
  184.7 4.5 %collective-permute-start.39 = (bf16[128,1024]{1,0:T(8,128)(2,1)S(1)}, bf16[128,1024]{1,0:T(8,128)(2,1)S(1)}, u32[]{:S(2)}, u32[]{:S(2)}) collective-permute-start(bf16[128,1024]{1,0:T(8,128)(2,1)S(1)} %bitcast.79), channel_id=1, source_target_pairs={{0,4},{2,6},{12,8},{14,10},{1,5},{3,7},{13,9},{15,11},{16,20},{18,... | collective-permute-start | bytes 786440 | tf_op jit(solution)/shard_map/ppermute | solution.py:258
  197.4 4.1 %collective-permute-done.41.refs_3_ = bf16[128,1024]{1,0:T(8,128)(2,1)S(1)} collective-permute-done((bf16[128,1024]{1,0:T(8,128)(2,1)S(1)}, bf16[128,1024]{1,0:T(8,128)(2,1)S(1)}, u32[]{:S(2)}, u32[]{:S(2)}) %collective-permute-start.41) | collective-permute-done | bytes 262176 | tf_op jit(solution)/shard_map/ppermute | solution.py:258
  203.8 2.7 %collective-permute-done.28.refs_2_ = bf16[128,1024]{1,0:T(8,128)(2,1)S(1)} collective-permute-done((bf16[128,1024]{1,0:T(8,128)(2,1)S(1)}, bf16[128,1024]{1,0:T(8,128)(2,1)S(1)}, u32[]{:S(2)}, u32[]{:S(2)}) %collective-permute-start.28) | collective-permute-done | bytes 262176 | tf_op jit(solution)/shard_map/ppermute | solution.py:258
  211.6 23.7 %collective-permute-start.45 = (bf16[256,512]{1,0:T(8,128)(2,1)S(1)}, bf16[256,512]{1,0:T(8,128)(2,1)S(1)}, u32[]{:S(2)}, u32[]{:S(2)}) collective-permute-start(bf16[256,512]{1,0:T(8,128)(2,1)S(1)} %add_convert_fusion), channel_id=1, source_target_pairs={{0,4},{2,6},{4,0},{6,2},{8,12},{10,14},{12,8},{14,10},{1,5},{3,7},... | collective-permute-start | bytes 786440 | tf_op jit(solution)/shard_map/ppermute | solution.py:258
  235.4 2.7 %collective-permute-start.43 = (bf16[256,512]{1,0:T(8,128)(2,1)S(1)}, bf16[256,512]{1,0:T(8,128)(2,1)S(1)}, u32[]{:S(2)}, u32[]{:S(2)}) collective-permute-start(bf16[256,512]{1,0:T(8,128)(2,1)S(1)} %add_convert_fusion.1), channel_id=1, source_target_pairs={{0,4},{2,6},{4,0},{6,2},{8,12},{10,14},{12,8},{14,10},{1,5},{3,7},... | collective-permute-start | bytes 786440 | tf_op jit(solution)/shard_map/ppermute | solution.py:258
  238.2 2.7 %collective-permute-start.34 = (bf16[256,512]{1,0:T(8,128)(2,1)S(1)}, bf16[256,512]{1,0:T(8,128)(2,1)S(1)}, u32[]{:S(2)}, u32[]{:S(2)}) collective-permute-start(bf16[256,512]{1,0:T(8,128)(2,1)S(1)} %add_convert_fusion.2), channel_id=1, source_target_pairs={{0,4},{2,6},{4,0},{6,2},{8,12},{10,14},{12,8},{14,10},{1,5},{3,7},... | collective-permute-start | bytes 786440 | tf_op jit(solution)/shard_map/ppermute | solution.py:258
  (119 shorter events, 68.1 us)
Async XLA Ops:
  0.0 33.2 %collective-permute-start.19 = (bf16[256,2048]{1,0:T(8,128)(2,1)}, bf16[256,2048]{1,0:T(8,128)(2,1)S(1)}, u32[]{:S(2)}, u32[]{:S(2)}) collective-permute-start(bf16[256,2048]{1,0:T(8,128)(2,1)} %x_ref.1), channel_id=1, source_target_pairs={{0,4},{2,6},{4,0},{6,2},{8,12},{10,14},{12,8},{14,10},{1,5},{3,7},... | collective-permute-start | bytes 3145736 | tf_op jit(solution)/shard_map/ppermute | solution.py:258
  3.1 47.1 %collective-permute-start.1 = (bf16[2,2048,256]{2,1,0:T(8,128)(2,1)}, bf16[2,2048,256]{2,1,0:T(8,128)(2,1)S(1)}, u32[]{:S(2)}, u32[]{:S(2)}) collective-permute-start(bf16[2,2048,256]{2,1,0:T(8,128)(2,1)} %refs_5_.7), channel_id=1, source_target_pairs={{0,1},{1,0},{2,3},{3,2},{4,5},{5,4},{6,7},{7,6},{8,9},{9,8},{10,11... | collective-permute-start | bytes 6291464 | tf_op jit(solution)/shard_map/ppermute | solution.py:264
  3.1 48.4 %collective-permute-start.2 = (bf16[2,2048,256]{2,1,0:T(8,128)(2,1)}, bf16[2,2048,256]{2,1,0:T(8,128)(2,1)}, u32[]{:S(2)}, u32[]{:S(2)}) collective-permute-start(bf16[2,2048,256]{2,1,0:T(8,128)(2,1)} %refs_6_.3), channel_id=1, source_target_pairs={{0,1},{1,0},{2,3},{3,2},{4,5},{5,4},{6,7},{7,6},{8,9},{9,8},{10,11... | collective-permute-start | bytes 6291464 | tf_op jit(solution)/shard_map/ppermute | solution.py:264
  3.6 49.2 %collective-permute-start.3 = (bf16[2,256,2048]{2,1,0:T(8,128)(2,1)}, bf16[2,256,2048]{2,1,0:T(8,128)(2,1)}, u32[]{:S(2)}, u32[]{:S(2)}) collective-permute-start(bf16[2,256,2048]{2,1,0:T(8,128)(2,1)} %refs_7_.3), channel_id=1, source_target_pairs={{0,1},{1,0},{2,3},{3,2},{4,5},{5,4},{6,7},{7,6},{8,9},{9,8},{10,11... | collective-permute-start | bytes 6291464 | tf_op jit(solution)/shard_map/ppermute | solution.py:264
  4.9 20.9 %collective-permute-start.22 = (f32[4,256]{1,0:T(4,128)S(1)}, f32[4,256]{1,0:T(4,128)S(1)}, u32[]{:S(2)}, u32[]{:S(2)}) collective-permute-start(f32[4,256]{1,0:T(4,128)S(1)} %pad_maximum_fusion.m_ref), channel_id=1, source_target_pairs={{12,4},{14,6},{0,8},{2,10},{13,5},{15,7},{1,9},{3,11},{28,20},{30,... | collective-permute-start | bytes 12296 | tf_op jit(solution)/shard_map/ppermute | solution.py:258
  43.4 82.1 %collective-permute-start.5 = (bf16[2048,256]{1,0:T(8,128)(2,1)S(1)}, bf16[2048,256]{1,0:T(8,128)(2,1)S(1)}, u32[]{:S(2)}, u32[]{:S(2)}) collective-permute-start(bf16[2048,256]{1,0:T(8,128)(2,1)S(1)} %copy-done.5), channel_id=1, source_target_pairs={{0,1},{1,0},{2,3},{3,2},{4,5},{5,4},{6,7},{7,6},{8,9},{9,8},{10,11... | collective-permute-start | bytes 3145736 | tf_op jit(solution)/shard_map/ppermute | solution.py:264
  50.2 76.1 %collective-permute-start.6 = (bf16[2048,256]{1,0:T(8,128)(2,1)S(1)}, bf16[2048,256]{1,0:T(8,128)(2,1)S(1)}, u32[]{:S(2)}, u32[]{:S(2)}) collective-permute-start(bf16[2048,256]{1,0:T(8,128)(2,1)S(1)} %copy-done.6), channel_id=1, source_target_pairs={{0,1},{1,0},{2,3},{3,2},{4,5},{5,4},{6,7},{7,6},{8,9},{9,8},{10,11... | collective-permute-start | bytes 3145736 | tf_op jit(solution)/shard_map/ppermute | solution.py:264
  50.2 51.3 %collective-permute-start.10 = (bf16[128,2048]{1,0:T(8,128)(2,1)S(1)}, bf16[128,2048]{1,0:T(8,128)(2,1)S(1)}, u32[]{:S(2)}, u32[]{:S(2)}) collective-permute-start(bf16[128,2048]{1,0:T(8,128)(2,1)S(1)} %get-tuple-element.40), channel_id=1, source_target_pairs={{4,0},{6,2},{8,12},{10,14},{5,1},{7,3},{9,13},{11,15},{20,16},{22,... | collective-permute-start | bytes 1572872 | tf_op jit(solution)/shard_map/ppermute | solution.py:258
  51.5 61.6 %collective-permute-start.11 = (bf16[128,2048]{1,0:T(8,128)(2,1)S(1)}, bf16[128,2048]{1,0:T(8,128)(2,1)S(1)}, u32[]{:S(2)}, u32[]{:S(2)}) collective-permute-start(bf16[128,2048]{1,0:T(8,128)(2,1)S(1)} %get-tuple-element.41), channel_id=1, source_target_pairs={{4,2},{6,0},{8,14},{10,12},{5,3},{7,1},{9,15},{11,13},{20,18},{22,... | collective-permute-start | bytes 1572872 | tf_op jit(solution)/shard_map/ppermute | solution.py:258
  52.8 60.3 %collective-permute-start.12 = (bf16[128,2048]{1,0:T(8,128)(2,1)S(1)}, bf16[128,2048]{1,0:T(8,128)(2,1)S(1)}, u32[]{:S(2)}, u32[]{:S(2)}) collective-permute-start(bf16[128,2048]{1,0:T(8,128)(2,1)S(1)} %get-tuple-element.42), channel_id=1, source_target_pairs={{4,6},{6,4},{8,10},{10,8},{5,7},{7,5},{9,11},{11,9},{20,22},{22,20... | collective-permute-start | bytes 1572872 | tf_op jit(solution)/shard_map/ppermute | solution.py:258
  101.4 22.8 %collective-permute-start = (bf16[128,2048]{1,0:T(8,128)(2,1)S(1)}, bf16[128,2048]{1,0:T(8,128)(2,1)S(1)}, u32[]{:S(2)}, u32[]{:S(2)}) collective-permute-start(bf16[128,2048]{1,0:T(8,128)(2,1)S(1)} %get-tuple-element.36), channel_id=1, source_target_pairs={{0,2},{2,0},{4,6},{6,4},{8,10},{10,8},{12,14},{14,12},{1,3},{3,1},... | collective-permute-start | bytes 1572872 | tf_op jit(solution)/shard_map/ppermute | solution.py:258
  113.1 45.5 %collective-permute-start.7 = (bf16[256,2048]{1,0:T(8,128)(2,1)S(1)}, bf16[256,2048]{1,0:T(8,128)(2,1)S(1)}, u32[]{:S(2)}, u32[]{:S(2)}) collective-permute-start(bf16[256,2048]{1,0:T(8,128)(2,1)S(1)} %copy-done.7), channel_id=1, source_target_pairs={{0,1},{1,0},{2,3},{3,2},{4,5},{5,4},{6,7},{7,6},{8,9},{9,8},{10,11... | collective-permute-start | bytes 3145736 | tf_op jit(solution)/shard_map/ppermute | solution.py:264
  113.1 34.7 %collective-permute-start.24 = (bf16[128,2048]{1,0:T(8,128)(2,1)S(1)}, bf16[128,2048]{1,0:T(8,128)(2,1)S(1)}, u32[]{:S(2)}, u32[]{:S(2)}) collective-permute-start(bf16[128,2048]{1,0:T(8,128)(2,1)S(1)} %get-tuple-element.52), channel_id=1, source_target_pairs={{4,0},{6,2},{8,12},{10,14},{5,1},{7,3},{9,13},{11,15},{20,16},{22,... | collective-permute-start | bytes 1572872 | tf_op jit(solution)/shard_map/ppermute | solution.py:258
  124.2 26.6 %collective-permute-start.25 = (bf16[128,2048]{1,0:T(8,128)(2,1)S(1)}, bf16[128,2048]{1,0:T(8,128)(2,1)S(1)}, u32[]{:S(2)}, u32[]{:S(2)}) collective-permute-start(bf16[128,2048]{1,0:T(8,128)(2,1)S(1)} %get-tuple-element.53), channel_id=1, source_target_pairs={{4,2},{6,0},{8,14},{10,12},{5,3},{7,1},{9,15},{11,13},{20,18},{22,... | collective-permute-start | bytes 1572872 | tf_op jit(solution)/shard_map/ppermute | solution.py:258
  125.5 26.7 %collective-permute-start.26 = (bf16[128,2048]{1,0:T(8,128)(2,1)S(1)}, bf16[128,2048]{1,0:T(8,128)(2,1)S(1)}, u32[]{:S(2)}, u32[]{:S(2)}) collective-permute-start(bf16[128,2048]{1,0:T(8,128)(2,1)S(1)} %get-tuple-element.54), channel_id=1, source_target_pairs={{4,6},{6,4},{8,10},{10,8},{5,7},{7,5},{9,11},{11,9},{20,22},{22,20... | collective-permute-start | bytes 1572872 | tf_op jit(solution)/shard_map/ppermute | solution.py:258
  126.2 20.2 %collective-permute-start.36 = (bf16[128,1024]{1,0:T(8,128)(2,1)S(1)}, bf16[128,1024]{1,0:T(8,128)(2,1)S(1)}, u32[]{:S(2)}, u32[]{:S(2)}) collective-permute-start(bf16[128,1024]{1,0:T(8,128)(2,1)S(1)} %bitcast.85), channel_id=1, source_target_pairs={{0,2},{2,0},{12,14},{14,12},{1,3},{3,1},{13,15},{15,13},{16,18},{1... | collective-permute-start | bytes 786440 | tf_op jit(solution)/shard_map/ppermute | solution.py:258
  160.2 24.5 %collective-permute-start.4 = (bf16[128,2048]{1,0:T(8,128)(2,1)S(1)}, bf16[128,2048]{1,0:T(8,128)(2,1)S(1)}, u32[]{:S(2)}, u32[]{:S(2)}) collective-permute-start(bf16[128,2048]{1,0:T(8,128)(2,1)S(1)} %bitcast.63), channel_id=1, source_target_pairs={{0,2},{2,0},{4,6},{6,4},{8,10},{10,8},{12,14},{14,12},{1,3},{3,1},... | collective-permute-start | bytes 1572872 | tf_op jit(solution)/shard_map/ppermute | solution.py:258
  161.4 28.8 %collective-permute-start.40 = (bf16[128,1024]{1,0:T(8,128)(2,1)S(1)}, bf16[128,1024]{1,0:T(8,128)(2,1)S(1)}, u32[]{:S(2)}, u32[]{:S(2)}) collective-permute-start(bf16[128,1024]{1,0:T(8,128)(2,1)S(1)} %bitcast.84), channel_id=1, source_target_pairs={{0,2},{2,0},{12,14},{14,12},{1,3},{3,1},{13,15},{15,13},{16,18},{1... | collective-permute-start | bytes 786440 | tf_op jit(solution)/shard_map/ppermute | solution.py:258
  165.0 37.2 %collective-permute-start.27 = (bf16[128,2048]{1,0:T(8,128)(2,1)S(1)}, bf16[128,2048]{1,0:T(8,128)(2,1)S(1)}, u32[]{:S(2)}, u32[]{:S(2)}) collective-permute-start(bf16[128,2048]{1,0:T(8,128)(2,1)S(1)} %bitcast.61), channel_id=1, source_target_pairs={{4,6},{6,4},{8,10},{10,8},{5,7},{7,5},{9,11},{11,9},{20,22},{22,20... | collective-permute-start | bytes 1572872 | tf_op jit(solution)/shard_map/ppermute | solution.py:258
  196.7 44.3 %collective-permute-start.38 = (bf16[256,1024]{1,0:T(8,128)(2,1)S(1)}, bf16[256,1024]{1,0:T(8,128)(2,1)S(1)}, u32[]{:S(2)}, u32[]{:S(2)}) collective-permute-start(bf16[256,1024]{1,0:T(8,128)(2,1)S(1)} %combine_piece.9), channel_id=1, source_target_pairs={{4,8},{6,10},{8,4},{10,6},{5,9},{7,11},{9,5},{11,7},{20,24},{22,26... | collective-permute-start | bytes 1572872 | tf_op jit(solution)/shard_map/ppermute | solution.py:258
  201.5 44.6 %collective-permute-start.17 = (bf16[256,1024]{1,0:T(8,128)(2,1)S(1)}, bf16[256,1024]{1,0:T(8,128)(2,1)S(1)}, u32[]{:S(2)}, u32[]{:S(2)}) collective-permute-start(bf16[256,1024]{1,0:T(8,128)(2,1)S(1)} %combine_piece.6), channel_id=1, source_target_pairs={{4,8},{6,10},{8,4},{10,6},{5,9},{7,11},{9,5},{11,7},{20,24},{22,26... | collective-permute-start | bytes 1572872 | tf_op jit(solution)/shard_map/ppermute | solution.py:258
  209.7 25.7 %collective-permute-start.33 = (bf16[256,512]{1,0:T(8,128)(2,1)S(1)}, bf16[256,512]{1,0:T(8,128)(2,1)S(1)}, u32[]{:S(2)}, u32[]{:S(2)}) collective-permute-start(bf16[256,512]{1,0:T(8,128)(2,1)S(1)} %combine_piece.8), channel_id=1, source_target_pairs={{4,8},{6,10},{8,4},{10,6},{5,9},{7,11},{9,5},{11,7},{20,24},{22,26... | collective-permute-start | bytes 786440 | tf_op jit(solution)/shard_map/ppermute | solution.py:258
  210.8 27.4 %collective-permute-start.31 = (bf16[256,512]{1,0:T(8,128)(2,1)S(1)}, bf16[256,512]{1,0:T(8,128)(2,1)S(1)}, u32[]{:S(2)}, u32[]{:S(2)}) collective-permute-start(bf16[256,512]{1,0:T(8,128)(2,1)S(1)} %combine_piece.7), channel_id=1, source_target_pairs={{4,8},{6,10},{8,4},{10,6},{5,9},{7,11},{9,5},{11,7},{20,24},{22,26... | collective-permute-start | bytes 786440 | tf_op jit(solution)/shard_map/ppermute | solution.py:258
  211.6 30.9 %collective-permute-start.45 = (bf16[256,512]{1,0:T(8,128)(2,1)S(1)}, bf16[256,512]{1,0:T(8,128)(2,1)S(1)}, u32[]{:S(2)}, u32[]{:S(2)}) collective-permute-start(bf16[256,512]{1,0:T(8,128)(2,1)S(1)} %add_convert_fusion), channel_id=1, source_target_pairs={{0,4},{2,6},{4,0},{6,2},{8,12},{10,14},{12,8},{14,10},{1,5},{3,7},... | collective-permute-start | bytes 786440 | tf_op jit(solution)/shard_map/ppermute | solution.py:258
  (31 other events, 370.2 us)
